TPU v7x, 32 devices: a whole 2x2x4 slice. The times are simulated.
32 devices in a mesh: sp: 8 (over z, y), tp: 4 (over x, core).
Axes of the slice: x: 2, y: 2, z: 4, core: 2. Of those that a mesh axis runs over, the one named last changes fastest.
Arguments:
- resid_stream: bfloat16 [3072, 2048], P('sp'), may hold values from -6 to 6
- q_latent: bfloat16 [3072, 512], P('sp'), may hold values from -6 to 6
- kv_latent: bfloat16 [3072, 256], P('sp'), may hold values from -6 to 6
- rope_key: bfloat16 [3072, 64], P('sp'), may hold values from -6 to 6
- doc_ids: int32 [3072], P('sp'), may hold values from 0 to 3, as said below
- q_gain: float32 [512], replicated, may hold values from 1.5 to 64
- kv_gain: float32 [256], replicated, may hold values from 0.1 to 1.9
- w_query: bfloat16 [512, 3072], P(None, 'tp'), may hold values from -0.25 to 0.25
- w_key: bfloat16 [256, 2048], P(None, 'tp'), may hold values from -0.375 to 0.375
- w_value: bfloat16 [256, 2048], P(None, 'tp'), may hold values from -0.375 to 0.375
- w_out: bfloat16 [2048, 2048], replicated, may hold values from -0.5 to 0.5
- mix_gain: float32 [2048], replicated, may hold values from 0.1 to 1.9
- w_gate: bfloat16 [2048, 5632], P('sp', 'tp'), may hold values from -0.125 to 0.125
- w_up: bfloat16 [2048, 5632], P('sp', 'tp'), may hold values from -0.125 to 0.125
- w_down: bfloat16 [5632, 2048], P('tp', 'sp'), may hold values from -0.3125 to 0.3125
- out_gain: float32 [2048], replicated, may hold values from 0.1 to 1.9
Outputs:
- layer_out: bfloat16 [3072, 2048], P(('sp', 'tp'))
Inputs may be any that keep to these rules, and one draw needn't show every extreme that they name: `doc_ids`: document numbers never fall along the sequence; every document has 1 to 2304 positions and one has exactly 2304.
All inputs are finite; a program needn't handle non-finite values.
Results may differ from a plain program's by a relative error of at most 0.02.
The roundings to bfloat16 on the way count: a program that leaves them out, or rounds other values in their place, can miss the bound.
Values may be sent and summed in bfloat16 or wider, within the bound.
A program may use at most 128 MiB of HBM per device.

v0:
```python
import functools
import math

import jax
import jax.numpy as jnp
from jax import lax
from jax.experimental import pallas as pl
from jax.experimental.pallas import tpu as pltpu
from jax.sharding import PartitionSpec as P

NOPE = 128
RD = 64
VD = 128


eps_norm = 1e-05
rope_theta = 10000.0
resid_alpha = 8.0**0.25
key_span = 2048


def rope_angles(positions):
    frequency = rope_theta ** (-jnp.arange(0, RD, 2, dtype=jnp.float32) / RD)
    angles = positions.astype(jnp.float32)[:, None] * frequency[None, :]
    return (jnp.cos(angles), jnp.sin(angles))


def rotate(values, cos_table, sin_table):
    half_width = values.shape[-1] // 2
    first_half = values[..., :half_width]
    second_half = values[..., half_width:]
    return jnp.concatenate(
        [
            first_half * cos_table - second_half * sin_table,
            second_half * cos_table + first_half * sin_table,
        ],
        axis=-1,
    )


def rms_scaled(latent, scaling):
    widened = latent.astype(jnp.float32)
    inverse = lax.rsqrt(jnp.mean(widened * widened, axis=-1, keepdims=True) + eps_norm)
    return (widened * inverse * scaling).astype(jnp.bfloat16)


def layer_scaled(stream, scaling):
    centre = stream - jnp.mean(stream, axis=-1, keepdims=True)
    spread = jnp.mean(centre * centre, axis=-1, keepdims=True)
    return centre * lax.rsqrt(spread + eps_norm) * scaling


def fold_in_blocks(carried, piece_part, attend_fn):
    piece_rows = piece_part[0].shape[0]
    if piece_rows > key_span and piece_rows % key_span == 0:

        def one_block(inner, block_index):
            sliced = tuple(
                (
                    lax.dynamic_slice_in_dim(
                        member, (block_index * key_span).astype(jnp.int32), key_span, 0
                    )
                    for member in piece_part
                )
            )
            return (attend_fn(inner, sliced), None)

        outcome = lax.scan(one_block, carried, jnp.arange(piece_rows // key_span, dtype=jnp.int32))
        return outcome[0]
    return attend_fn(carried, piece_part)


class Ring:
    def __init__(self, blocks):
        self.count = lax.axis_size("sp")
        ring = list(range(0, self.count, 2)) + list(range(1, self.count, 2))[::-1]
        places = [ring.index(i) for i in range(self.count)]
        self.place = jnp.array(places, jnp.int32)[lax.axis_index("sp")]
        self.ring_of = jnp.array(ring, jnp.int32)
        self.right = [(ring[i], ring[(i + 1) % self.count]) for i in range(self.count)]
        self.left = [(after, before) for before, after in self.right]
        self.pieces = [[(lax.axis_index("sp"), block)] for block in blocks]
        self.flying = [(block, block) for block in blocks]
        self.step = 0

    def owner(self, distance):
        return self.ring_of[(self.place + distance) % self.count]

    def hop(self):
        self.step += 1
        self.send()

    def send(self):
        if self.step < self.count // 2:
            self.flying = [
                (lax.ppermute(one, "sp", self.right), lax.ppermute(two, "sp", self.left))
                for one, two in self.flying
            ]
        elif self.step == self.count // 2:
            self.flying = [
                (
                    lax.ppermute(one[: one.shape[0] // 2], "sp", self.right),
                    lax.ppermute(two[two.shape[0] // 2 :], "sp", self.left),
                )
                for one, two in self.flying
            ]

    def land(self, *values):
        if self.step <= self.count // 2:
            if values:
                values, self.flying = lax.optimization_barrier((values, self.flying))
            for pieces, (one, two) in zip(self.pieces, self.flying):
                if self.step < self.count // 2:
                    pieces.append((self.owner(-self.step), one))
                    pieces.append((self.owner(self.step), two))
                else:
                    pieces.append((self.owner(self.step), jnp.concatenate([one, two])))
        return values


def body(
    resid_stream,
    q_latent,
    kv_latent,
    rope_key,
    doc_ids,
    q_gain,
    kv_gain,
    w_query,
    w_key,
    w_value,
    w_out,
    mix_gain,
    w_gate,
    w_up,
    w_down,
    out_gain,
):
    tok_rows = q_latent.shape[0]
    head_count = w_key.shape[1] // NOPE
    tp_count = lax.axis_size("tp")
    part_rows = tok_rows // tp_count
    tp_index = lax.axis_index("tp")
    gate_ring = Ring([jnp.concatenate([w_gate, w_up], axis=1)])
    down_ring = Ring([w_down])
    gate_ring.hop()
    positions = lax.axis_index("sp") * tok_rows + jnp.arange(tok_rows, dtype=jnp.int32)
    cos_table, sin_table = rope_angles(positions)
    q_normed = rms_scaled(q_latent, q_gain)
    queries = jnp.dot(q_normed, w_query, preferred_element_type=jnp.float32).reshape(
        tok_rows, head_count, NOPE + RD
    )
    query_nope = queries[:, :, :NOPE].astype(jnp.bfloat16)
    query_rope = rotate(queries[:, :, NOPE:], cos_table[:, None, :], sin_table[:, None, :]).astype(
        jnp.bfloat16
    )
    kv_normed = rms_scaled(kv_latent, kv_gain)
    key_rot = rotate(rope_key.astype(jnp.float32), cos_table, sin_table).astype(jnp.bfloat16)
    score_scale = (NOPE + RD) ** (-0.5)

    def attend_rows(carried, piece_part, between=lambda value: value):
        row_top, denom_sum, accum_out = carried
        key_piece, value_piece, rot_piece, doc_piece = piece_part
        piece_rows = key_piece.shape[0]
        keys_heads = key_piece.reshape(piece_rows, head_count, NOPE)
        values_heads = value_piece.reshape(piece_rows, head_count, VD)
        scores = jnp.einsum(
            "qhd,khd->hqk", query_nope, keys_heads, preferred_element_type=jnp.float32
        )
        scores = (
            scores
            + jnp.einsum("qhd,kd->hqk", query_rope, rot_piece, preferred_element_type=jnp.float32)
        ) * score_scale
        same_doc = (doc_ids[:, None] == doc_piece[None, :])[None]
        masked = jnp.where(same_doc, scores, -1e30)
        new_top = jnp.maximum(row_top, jnp.max(masked, axis=-1))
        weights = jnp.where(same_doc, jnp.exp(masked - new_top[:, :, None]), 0.0)
        factor = jnp.exp(row_top - new_top)
        denom_sum = denom_sum * factor + jnp.sum(weights, axis=-1)
        weights = between(weights.astype(jnp.bfloat16))
        update = jnp.einsum(
            "hqk,khd->qhd", weights, values_heads, preferred_element_type=jnp.float32
        )
        accum_out = accum_out * jnp.transpose(factor)[:, :, None] + update
        return (new_top, denom_sum, accum_out)

    initial = (
        jnp.full((head_count, tok_rows), -1e30, jnp.float32),
        jnp.zeros((head_count, tok_rows), jnp.float32),
        jnp.zeros((tok_rows, head_count, VD), jnp.float32),
    )

    def project_rows(carried, piece_part, between=lambda value: value):
        latent_piece, rot_piece, doc_piece = piece_part
        key_piece = jnp.dot(latent_piece, w_key, preferred_element_type=jnp.float32).astype(
            jnp.bfloat16
        )
        value_piece = jnp.dot(latent_piece, w_value, preferred_element_type=jnp.float32).astype(
            jnp.bfloat16
        )
        return attend_rows(carried, (key_piece, value_piece, rot_piece, doc_piece), between)

    def next_hop(value):
        (value,) = gate_ring.land(value)
        gate_ring.hop()
        return value

    doc_lanes = jnp.broadcast_to(doc_ids.astype(jnp.bfloat16)[:, None], (tok_rows, RD))
    packed = jnp.concatenate([kv_normed, key_rot, doc_lanes], axis=1)
    packed_part = lax.dynamic_slice_in_dim(packed, tp_index * part_rows, part_rows, 0)
    packed_all = lax.all_gather(packed_part, ("sp", "tp"), axis=0, tiled=True)
    packed_all = next_hop(packed_all)
    kv_rank = kv_latent.shape[1]
    gathered = (
        packed_all[:, :kv_rank],
        packed_all[:, kv_rank : kv_rank + RD],
        packed_all[:, kv_rank + RD].astype(jnp.int32),
    )
    if packed_all.shape[0] > key_span and packed_all.shape[0] % key_span == 0:
        carried_out = fold_in_blocks(initial, gathered, project_rows)
    else:
        carried_out = project_rows(initial, gathered, next_hop)
    denom_sum = carried_out[1]
    attended = (
        (carried_out[2] / jnp.transpose(denom_sum)[:, :, None])
        .astype(jnp.bfloat16)
        .reshape(tok_rows, head_count * VD)
    )
    heads_rows = lax.all_to_all(attended, "tp", split_axis=0, concat_axis=1, tiled=True)
    mixer_out = jnp.dot(heads_rows, w_out, preferred_element_type=jnp.float32)
    own_resid = lax.dynamic_slice_in_dim(resid_stream, tp_index * part_rows, part_rows, 0)
    own_normed = layer_scaled(
        resid_alpha * own_resid.astype(jnp.float32) + mixer_out, mix_gain
    ).astype(jnp.bfloat16)
    (own_normed,) = gate_ring.land(own_normed)
    down_ring.hop()
    gate_ring.hop()
    normed_rows = lax.all_gather(own_normed, "tp", axis=0, tiled=True)
    (normed_rows,) = down_ring.land(normed_rows)
    down_ring.hop()
    gate_ring.land()
    while gate_ring.step < gate_ring.count // 2:
        gate_ring.hop()
        gate_ring.land()
    gate_sum = None
    for owner, piece in gate_ring.pieces[0]:
        rows = lax.dynamic_slice_in_dim(normed_rows, owner * piece.shape[0], piece.shape[0], 1)
        term = jnp.dot(rows, piece, preferred_element_type=jnp.float32)
        gate_sum = term if gate_sum is None else gate_sum + term
    width = w_gate.shape[1]
    hidden = (jax.nn.silu(gate_sum[:, :width]) * gate_sum[:, width:]).astype(jnp.bfloat16)
    (hidden,) = down_ring.land(hidden)
    while down_ring.step < down_ring.count // 2:
        down_ring.hop()
        down_ring.land()
    down = down_ring.pieces[0]
    ffn_sum = jnp.zeros((part_rows, resid_stream.shape[1]), jnp.float32)
    for part, group in enumerate((down[: len(down) // 2], down[len(down) // 2 :])):
        pieces = [piece for _, piece in group]
        if part == 0:
            pieces = [jnp.concatenate(pieces, axis=1)]
        terms = [
            jnp.dot(hidden, piece, preferred_element_type=jnp.float32).astype(jnp.bfloat16)
            for piece in pieces
        ]
        partial = jnp.concatenate(terms, axis=1)
        swapped = lax.all_to_all(
            partial.reshape(tp_count, part_rows, -1), "tp", split_axis=0, concat_axis=0, tiled=True
        )
        summed = jnp.sum(swapped.astype(jnp.float32), axis=0)
        columns = w_down.shape[1]
        for at, (owner, _) in enumerate(group):
            ffn_sum = lax.dynamic_update_slice_in_dim(
                ffn_sum, summed[:, at * columns : (at + 1) * columns], owner * columns, 1
            )
    layer_out = layer_scaled(
        resid_alpha * own_normed.astype(jnp.float32) + 0.5 * ffn_sum, out_gain
    ).astype(jnp.bfloat16)
    return layer_out


CORES = 2
LANES = 128
MESH = pl.DeviceIdType.MESH
log2_e = math.log2(math.e)


def rms_rows(latent, scaling):
    widened = latent.astype(jnp.float32)
    inverse = lax.rsqrt(jnp.mean(widened * widened, axis=-1, keepdims=True) + eps_norm)
    return (widened * inverse * scaling).astype(jnp.bfloat16)


def near_order(step, z, nz):
    paired = 2 * jnp.minimum(z, nz - 1 - z)
    half = (step + 1) // 2
    close = jnp.where(step % 2 == 1, z - half, z + half)
    far = step - paired // 2
    wide = jnp.where(z < nz - 1 - z, z + far, z - far)
    return jnp.where(step <= paired, close, wide)


def layer_kernel(
    nz,
    ny,
    heads,
    q_latent,
    kv_latent,
    rope_key,
    cos_ref,
    sin_ref,
    q_side,
    k_side,
    q_gain,
    kv_gain,
    mix_gain,
    out_gain,
    w_query,
    w_key,
    w_value,
    resid,
    w_out,
    w_gate,
    w_up,
    w_down,
    out_ref,
    packed,
    queries,
    keys,
    vals,
    scores,
    top_ref,
    den_ref,
    acc_ref,
    attended,
    head_rows,
    out_weights,
    own_resid,
    gate_w,
    up_w,
    down_w,
    rows_all,
    hidden,
    part,
    core_part,
    x_stage,
    x_part,
    z_stage,
    up_part,
    dn_part,
    loc_sem,
    kvz_s,
    kvz_r,
    kvy_s,
    kvy_r,
    kvc_s,
    kvc_r,
    wz_s,
    wz_r,
    wy_s,
    wy_r,
    tp_s,
    tp_r,
    up_s,
    dn_s,
    z_r,
    x_s,
    x_r,
    c_s,
    c_r,
    crs_s,
    crs_r,
    xrs_s,
    xrs_r,
    zch_s,
    zup_r,
    zdn_r,
):
    sp = lax.axis_index("sp")
    tp = lax.axis_index("tp")
    z, y = sp // ny, sp % ny
    x, c = tp // CORES, tp % CORES
    tok = q_latent.shape[0]
    half = tok // CORES
    quarter = out_ref.shape[0]
    tp_count = tok // quarter
    depth = w_gate.shape[0]
    wide = gate_w.shape[1]
    ff = w_gate.shape[1]
    model = out_ref.shape[1]
    total = packed.shape[0]
    rank = kv_latent.shape[1]

    def at(zz=None, yy=None, xx=None, cc=None):
        zz = z if zz is None else zz
        yy = y if yy is None else yy
        xx = x if xx is None else xx
        cc = c if cc is None else cc
        return (zz * ny + yy, xx * CORES + cc)

    def remote(src, dst, send, recv, where):
        return pltpu.make_async_remote_copy(
            src_ref=src,
            dst_ref=dst,
            send_sem=send,
            recv_sem=recv,
            device_id=where,
            device_id_type=MESH,
        )

    y_mate = at(yy=1 - y)
    x_mate = at(xx=1 - x)
    c_mate = at(cc=1 - c)
    diagonal = at(xx=1 - x, cc=1 - c)
    z_mates = [at(zz=(z + s) % nz) for s in range(1, nz)]

    def piece_start(zz):
        return pl.multiple_of(jnp.minimum(zz * wide, ff - wide), LANES)

    def weight_slots(src_sp):
        rows = pl.ds(pl.multiple_of(src_sp * depth, depth), depth)
        return (gate_w.at[rows, :], up_w.at[rows, :], down_w.at[:, rows])

    def weight_sources(zz):
        lanes = pl.ds(piece_start(zz), wide)
        rows = pl.ds(piece_start(zz), wide)
        return (w_gate.at[:, lanes], w_up.at[:, lanes], w_down.at[rows, :])

    local = [
        pltpu.make_async_copy(src, dst, loc_sem.at[i])
        for i, (src, dst) in enumerate(zip(weight_sources(z), weight_slots(sp)))
    ]
    local.append(pltpu.make_async_copy(w_out, out_weights, loc_sem.at[3]))
    local.append(
        pltpu.make_async_copy(
            resid.at[pl.ds(pl.multiple_of(tp * quarter, quarter), quarter), :],
            own_resid,
            loc_sem.at[4],
        )
    )
    for one in local:
        one.start()

    kv_normed = rms_rows(kv_latent[...], kv_gain[...])
    cos_t, sin_t = cos_ref[...], sin_ref[...]

    def turn(values):
        swapped = jnp.concatenate([values[:, RD // 2 :], values[:, : RD // 2]], axis=1)
        return values * cos_t + swapped * sin_t

    key_rot = turn(rope_key[...].astype(jnp.float32))
    tail_lanes = jnp.concatenate([key_rot, k_side[...].astype(jnp.float32)], axis=1)
    own_at = pl.multiple_of(sp * tok, tok)
    packed[pl.ds(own_at, tok), :rank] = kv_normed
    packed[pl.ds(own_at, tok), rank:] = tail_lanes.astype(jnp.bfloat16)

    barrier = pltpu.get_barrier_semaphore()
    mates = z_mates + [y_mate, x_mate, c_mate, diagonal]
    for mate in mates:
        pl.semaphore_signal(barrier, inc=1, device_id=mate, device_id_type=MESH)
    pl.semaphore_wait(barrier, len(mates))

    sends = []

    def begin(copy):
        copy.start()
        sends.append(copy)

    def half_of(src_sp, cc):
        return packed.at[pl.ds(pl.multiple_of(src_sp * tok + cc * half, half), half), :]

    own_half = half_of(sp, c)
    for s in range(1, nz):
        begin(remote(own_half, own_half, kvz_s.at[s - 1], kvz_r.at[s - 1], z_mates[s - 1]))
    begin(remote(own_half, own_half, kvy_s.at[0], kvy_r.at[0], y_mate))
    for s in range(1, nz):
        slots = weight_slots(sp)
        for m, src in enumerate(weight_sources((z + s) % nz)):
            begin(remote(src, slots[m], wz_s.at[s - 1, m], wz_r.at[s - 1, m], z_mates[s - 1]))

    q_normed = rms_rows(q_latent[...], q_gain[...])
    for h in range(heads):
        wide_q = jnp.dot(
            q_normed,
            w_query[:, h * (NOPE + RD) : (h + 1) * (NOPE + RD)],
            preferred_element_type=jnp.float32,
        )
        rest = jnp.concatenate([turn(wide_q[:, NOPE:]), q_side[...].astype(jnp.float32)], axis=1)
        queries[h, :, :NOPE] = wide_q[:, :NOPE].astype(jnp.bfloat16)
        queries[h, :, NOPE:] = rest.astype(jnp.bfloat16)

    def source(s):
        return ((z + nz - s) % nz) * ny + y

    def source_y(s):
        return ((z + nz - s) % nz) * ny + (1 - y)

    for s in range(1, nz):
        block = half_of(source(s), c)
        remote(block, block, kvz_s.at[s - 1], kvz_r.at[s - 1], z_mates[s - 1]).wait_recv()
        begin(remote(block, block, kvy_s.at[s], kvy_r.at[s], y_mate))
        begin(remote(block, block, kvc_s.at[s - 1], kvc_r.at[s - 1], c_mate))
    slots = weight_slots(sp)
    for m in range(3):
        local[m].wait()
        begin(remote(slots[m], slots[m], wy_s.at[0, m], wy_r.at[0, m], y_mate))
    for s in range(nz):
        block = half_of(source_y(s), c)
        remote(block, block, kvy_s.at[s], kvy_r.at[s], y_mate).wait_recv()
        begin(remote(block, block, kvc_s.at[nz - 1 + s], kvc_r.at[nz - 1 + s], c_mate))
    for s in range(1, nz):
        block = half_of(source(s), 1 - c)
        remote(block, block, kvc_s.at[s - 1], kvc_r.at[s - 1], c_mate).wait_recv()
    for s in range(nz):
        block = half_of(source_y(s), 1 - c)
        remote(block, block, kvc_s.at[nz - 1 + s], kvc_r.at[nz - 1 + s], c_mate).wait_recv()

    chunk = scores.shape[2]
    chunks = total // chunk
    scale = (NOPE + RD) ** (-0.5) * log2_e

    def one_head(h, carry):
        top_ref[...] = jnp.full_like(top_ref, -3.0e38)
        head_lanes = pl.ds(pl.multiple_of(h * NOPE, NOPE), NOPE)

        def score_chunk(k, inner):
            rows = pl.ds(pl.multiple_of(k * chunk, chunk), chunk)
            latent = packed[rows, :rank]
            keys[:, :NOPE] = jnp.dot(
                latent, w_key[:, head_lanes], preferred_element_type=jnp.float32
            ).astype(jnp.bfloat16)
            vals[rows, :] = jnp.dot(
                latent, w_value[:, head_lanes], preferred_element_type=jnp.float32
            ).astype(jnp.bfloat16)
            keys[:, NOPE:] = packed[rows, rank:]
            value = lax.dot_general(
                queries[h], keys[...], (((1,), (1,)), ((), ())), preferred_element_type=jnp.float32
            )
            scores[k] = value
            most = top_ref[...]
            for j in range(chunk // LANES):
                most = jnp.maximum(most, value[:, j * LANES : (j + 1) * LANES])
            top_ref[...] = most
            return inner

        lax.fori_loop(0, chunks, score_chunk, 0)
        top = jnp.max(top_ref[...], axis=1, keepdims=True)
        den_ref[...] = jnp.zeros_like(den_ref)
        acc_ref[...] = jnp.zeros_like(acc_ref)

        def weigh_chunk(k, inner):
            rows = pl.ds(pl.multiple_of(k * chunk, chunk), chunk)
            weights = jnp.exp2((scores[k] - top) * scale)
            denom = den_ref[...]
            for j in range(chunk // LANES):
                denom = denom + weights[:, j * LANES : (j + 1) * LANES]
            den_ref[...] = denom
            acc_ref[...] += jnp.dot(
                weights.astype(jnp.bfloat16), vals[rows, :], preferred_element_type=jnp.float32
            )
            return inner

        lax.fori_loop(0, chunks, weigh_chunk, 0)
        denom = jnp.sum(den_ref[...], axis=1, keepdims=True)
        attended[:, head_lanes] = (acc_ref[...] / denom).astype(jnp.bfloat16)
        return carry

    lax.fori_loop(0, heads, one_head, 0)

    def rows_of(peer):
        return attended.at[pl.ds(pl.multiple_of(peer * quarter, quarter), quarter), :]

    my_slot = head_rows.at[tp]
    tp_mates = [(1, c_mate), (2, x_mate), (3, diagonal)]
    tp_of = [x * CORES + 1 - c, (1 - x) * CORES + c, (1 - x) * CORES + 1 - c]
    for i in (2, 1, 0):
        begin(remote(rows_of(tp_of[i]), my_slot, tp_s.at[i], tp_r.at[i], tp_mates[i][1]))
    head_rows[tp] = attended[pl.ds(pl.multiple_of(tp * quarter, quarter), quarter), :]

    def pass_weights(s):
        got = weight_slots(source(s))
        for m in range(3):
            remote(got[m], got[m], wz_s.at[s - 1, m], wz_r.at[s - 1, m], z_mates[s - 1]).wait_recv()
            begin(remote(got[m], got[m], wy_s.at[s, m], wy_r.at[s, m], y_mate))

    pass_weights(1)
    local[3].wait()
    local[4].wait()
    for i in range(3):
        remote(rows_of(tp_of[i]), head_rows.at[tp_of[i]], tp_s.at[i], tp_r.at[i], tp_mates[i][1]).wait_recv()
    span = head_rows.shape[2]
    mixed = resid_alpha * own_resid[...].astype(jnp.float32)
    for t in range(tp_count):
        mixed = mixed + jnp.dot(
            head_rows[t], out_weights[t * span : (t + 1) * span, :], preferred_element_type=jnp.float32
        )
    rows_all[z, x, c] = layer_scaled(mixed, mix_gain[...]).astype(jnp.bfloat16)

    delay = 1
    first = piece_start(z)
    stale = z * wide - first

    def z_sends(zz):
        block = rows_all.at[zz, x, c]
        return (
            (jnp.logical_and(zz <= z, z < nz - 1), remote(block, block, up_s.at[zz], z_r.at[zz], at(zz=jnp.minimum(z + 1, nz - 1)))),
            (jnp.logical_and(zz >= z, z > 0), remote(block, block, dn_s.at[zz], z_r.at[zz], at(zz=jnp.maximum(z - 1, 0)))),
        )

    def x_send(zz):
        block = rows_all.at[zz, x, c]
        return remote(block, block, x_s.at[zz], x_r.at[zz], x_mate)

    def c_send(zz, xx):
        block = rows_all.at[zz, xx, c]
        return remote(block, block, c_s.at[zz, xx], c_r.at[zz, xx], c_mate)

    def arrive_x(zz):
        block = rows_all.at[zz, 1 - x, c]
        remote(block, block, x_s.at[zz], x_r.at[zz], x_mate).wait_recv()

    def arrive_c(zz, xx):
        block = rows_all.at[zz, xx, 1 - c]
        remote(block, block, c_s.at[zz, xx], c_r.at[zz, xx], c_mate).wait_recv()

    def core_send(zz, xx):
        return remote(part.at[zz, xx, 1 - c], core_part.at[zz, xx], crs_s.at[zz, xx], crs_r.at[zz, xx], c_mate)

    def x_sum_send(zz):
        return remote(x_stage.at[zz], x_part.at[zz], xrs_s.at[zz], xrs_r.at[zz], x_mate)

    def up_sum_send(zz):
        return remote(z_stage.at[zz], up_part.at[zz], zch_s.at[zz], zup_r.at[zz], at(zz=jnp.minimum(z + 1, nz - 1)))

    def dn_sum_send(zz):
        return remote(z_stage.at[zz], dn_part.at[zz], zch_s.at[zz], zdn_r.at[zz], at(zz=jnp.maximum(z - 1, 0)))

    def pair_sum(zz, xx):
        return part[zz, xx, c].astype(jnp.float32) + core_part[zz, xx].astype(jnp.float32)

    def gather_step(step):
        zz = near_order(step, z, nz)

        @pl.when(step > 0)
        def _():
            block = rows_all.at[zz, x, c]
            remote(block, block, up_s.at[zz], z_r.at[zz], x_mate).wait_recv()

        for wanted, copy in z_sends(zz):
            pl.when(wanted)(copy.start)
        x_send(zz).start()
        c_send(zz, x).start()

    def mix_step(step):
        zz = near_order(step, z, nz)
        arrive_x(zz)
        c_send(zz, 1 - x).start()
        arrive_c(zz, x)
        arrive_c(zz, 1 - x)
        rows = 2 * CORES * quarter
        lanes = lax.broadcasted_iota(jnp.int32, (1, wide), 1)
        unit = rows_all[zz].reshape(rows, model)
        gate = jnp.dot(unit, gate_w[...], preferred_element_type=jnp.float32)
        up = jnp.dot(unit, up_w[...], preferred_element_type=jnp.float32)
        inner = jax.nn.silu(gate) * up
        hidden[...] = jnp.where(lanes >= stale, inner, 0.0).astype(jnp.bfloat16)
        cut = 512
        for n in range(model // cut):
            piece = jnp.dot(
                hidden[...], down_w[:, n * cut : (n + 1) * cut], preferred_element_type=jnp.float32
            ).astype(jnp.bfloat16)
            part[zz, :, :, :, n * cut : (n + 1) * cut] = piece.reshape(2, CORES, quarter, cut)
        core_send(zz, 1 - x).start()
        core_send(zz, x).start()
        core_send(zz, 1 - x).wait_recv()
        x_stage[zz] = pair_sum(zz, 1 - x).astype(jnp.bfloat16)
        x_sum_send(zz).start()

    def ready_sum(zz):
        core_send(zz, x).wait_recv()
        x_sum_send(zz).wait_recv()
        return pair_sum(zz, x) + x_part[zz].astype(jnp.float32)

    def chain_step(step):
        above = step - z - 1

        @pl.when(jnp.logical_and(above > z, above < nz))
        def _():
            z_stage[above] = ready_sum(above).astype(jnp.bfloat16)

            @pl.when(z > 0)
            def _():
                up_sum_send(above).wait_recv()
                z_stage[above] = (
                    z_stage[above].astype(jnp.float32) + up_part[above].astype(jnp.float32)
                ).astype(jnp.bfloat16)

            up_sum_send(above).start()

        mirrored = nz - 1 - z
        below_m = step - mirrored - 1
        below = nz - 1 - below_m

        @pl.when(jnp.logical_and(below_m > mirrored, below_m < nz))
        def _():
            z_stage[below] = ready_sum(below).astype(jnp.bfloat16)

            @pl.when(mirrored > 0)
            def _():
                dn_sum_send(below).wait_recv()
                z_stage[below] = (
                    z_stage[below].astype(jnp.float32) + dn_part[below].astype(jnp.float32)
                ).astype(jnp.bfloat16)

            dn_sum_send(below).start()

    gather_step(jnp.int32(0))
    for s in range(2, nz):
        pass_weights(s)
    for s in range(nz):
        got = weight_slots(source_y(s))
        for m in range(3):
            remote(got[m], got[m], wy_s.at[s, m], wy_r.at[s, m], y_mate).wait_recv()

    def one_step(step, carry):
        pl.when(step < nz)(lambda: gather_step(step))
        pl.when(step <= nz)(lambda: mix_step(step - 1))
        chain_step(step - delay)
        return carry

    lax.fori_loop(1, 2 * nz - 1 + delay, one_step, 0)

    ffn_sum = ready_sum(z)
    pl.when(z > 0)(up_sum_send(z).wait_recv)
    pl.when(z < nz - 1)(dn_sum_send(z).wait_recv)
    part_sum = ffn_sum + jnp.where(z > 0, up_part[z].astype(jnp.float32), 0.0)
    part_sum = part_sum + jnp.where(z < nz - 1, dn_part[z].astype(jnp.float32), 0.0)
    out_ref[...] = layer_scaled(
        resid_alpha * rows_all[z, x, c].astype(jnp.float32) + 0.5 * part_sum, out_gain[...]
    ).astype(jnp.bfloat16)

    for copy in sends:
        copy.wait_send()

    def drain(zz, carry):
        for wanted, copy in z_sends(zz):
            pl.when(wanted)(copy.wait_send)
        x_send(zz).wait_send()
        for xx in range(2):
            c_send(zz, xx).wait_send()
            core_send(zz, xx).wait_send()
        x_sum_send(zz).wait_send()
        pl.when(zz > z)(up_sum_send(zz).wait_send)
        pl.when(zz < z)(dn_sum_send(zz).wait_send)
        return carry

    lax.fori_loop(0, nz, drain, 0)


def fused_layer(
    sp_count,
    tp_count,
    resid_stream,
    q_latent,
    kv_latent,
    rope_key,
    doc_ids,
    q_gain,
    kv_gain,
    w_query,
    w_key,
    w_value,
    w_out,
    mix_gain,
    w_gate,
    w_up,
    w_down,
    out_gain,
):
    ny = tp_count // CORES
    nz = sp_count // ny
    tok = q_latent.shape[0]
    total = tok * sp_count
    quarter = tok // tp_count
    model = resid_stream.shape[1]
    heads = w_key.shape[1] // NOPE
    rank = kv_latent.shape[1]
    ff = w_gate.shape[1]
    wide = -(-ff // (LANES * nz)) * LANES
    chunk = 512
    positions = lax.axis_index("sp") * tok + jnp.arange(tok, dtype=jnp.int32)
    cos_table, sin_table = rope_angles(positions)
    cos_wide = jnp.concatenate([cos_table, cos_table], axis=1)
    sin_wide = jnp.concatenate([-sin_table, sin_table], axis=1)
    marks = (doc_ids[:, None] == jnp.arange(RD, dtype=jnp.int32)[None, :])
    k_side = jnp.where(marks, 1.0, 0.0).astype(jnp.bfloat16)
    q_side = jnp.where(marks, 0.0, -1e30).astype(jnp.bfloat16)
    vmem = pl.BlockSpec(memory_space=pltpu.VMEM)
    hbm = pl.BlockSpec(memory_space=pl.ANY)
    bf16, f32 = jnp.bfloat16, jnp.float32
    dma = pltpu.SemaphoreType.DMA
    scratch = [
        pltpu.VMEM((total, rank + 2 * RD), bf16),
        pltpu.VMEM((heads, tok, NOPE + 2 * RD), bf16),
        pltpu.VMEM((chunk, NOPE + 2 * RD), bf16),
        pltpu.VMEM((total, VD), bf16),
        pltpu.VMEM((total // chunk, tok, chunk), f32),
        pltpu.VMEM((tok, LANES), f32),
        pltpu.VMEM((tok, LANES), f32),
        pltpu.VMEM((tok, VD), f32),
        pltpu.VMEM((tok, heads * VD), bf16),
        pltpu.VMEM((tp_count, quarter, heads * VD), bf16),
        pltpu.VMEM(w_out.shape, bf16),
        pltpu.VMEM((quarter, model), bf16),
        pltpu.VMEM((model, wide), bf16),
        pltpu.VMEM((model, wide), bf16),
        pltpu.VMEM((wide, model), bf16),
        pltpu.VMEM((nz, 2, CORES, quarter, model), bf16),
        pltpu.VMEM((2 * CORES * quarter, wide), bf16),
        pltpu.VMEM((nz, 2, CORES, quarter, model), bf16),
        pltpu.VMEM((nz, 2, quarter, model), bf16),
        pltpu.VMEM((nz, quarter, model), bf16),
        pltpu.VMEM((nz, quarter, model), bf16),
        pltpu.VMEM((nz, quarter, model), bf16),
        pltpu.VMEM((nz, quarter, model), bf16),
        pltpu.VMEM((nz, quarter, model), bf16),
        dma((5,)),
        dma((nz - 1,)),
        dma((nz - 1,)),
        dma((nz,)),
        dma((nz,)),
        dma((2 * nz - 1,)),
        dma((2 * nz - 1,)),
        dma((nz - 1, 3)),
        dma((nz - 1, 3)),
        dma((nz, 3)),
        dma((nz, 3)),
        dma((3,)),
        dma((3,)),
        dma((nz,)),
        dma((nz,)),
        dma((nz,)),
        dma((nz,)),
        dma((nz,)),
        dma((nz, 2)),
        dma((nz, 2)),
        dma((nz, 2)),
        dma((nz, 2)),
        dma((nz,)),
        dma((nz,)),
        dma((nz,)),
        dma((nz,)),
        dma((nz,)),
    ]
    return pl.pallas_call(
        functools.partial(layer_kernel, nz, ny, heads),
        out_shape=jax.ShapeDtypeStruct((quarter, model), bf16),
        in_specs=[vmem] * 14 + [hbm] * 5,
        out_specs=vmem,
        scratch_shapes=scratch,
        compiler_params=pltpu.CompilerParams(
            collective_id=0, has_side_effects=True, vmem_limit_bytes=67043328
        ),
    )(
        q_latent,
        kv_latent,
        rope_key,
        cos_wide,
        sin_wide,
        q_side,
        k_side,
        q_gain[None, :],
        kv_gain[None, :],
        mix_gain[None, :],
        out_gain[None, :],
        w_query,
        w_key,
        w_value,
        resid_stream,
        w_out,
        w_gate,
        w_up,
        w_down,
    )


def solution(mesh):
    in_specs = (
        P("sp", None),
        P("sp", None),
        P("sp", None),
        P("sp", None),
        P("sp"),
        P(),
        P(),
        P(None, "tp"),
        P(None, "tp"),
        P(None, "tp"),
        P(),
        P(),
        P("sp", "tp"),
        P("sp", "tp"),
        P("tp", "sp"),
        P(),
    )
    out_specs = P(("sp", "tp"), None)
    if mesh.shape["tp"] == 2 * CORES:
        return jax.shard_map(
            functools.partial(fused_layer, mesh.shape["sp"], mesh.shape["tp"]),
            mesh=mesh,
            in_specs=in_specs,
            out_specs=out_specs,
            check_vma=False,
        )
    return jax.shard_map(body, mesh=mesh, in_specs=in_specs, out_specs=out_specs, check_vma=False)
```

profile of v0, /device:TPU:16, one launch (start us, length us, event | category | flops | bytes accessed | tf_op | source)
XLA Modules:
  0.0 207.7 jit_solution(249605087306879990)
XLA Ops:
  0.0 0.8 fusion
  0.8 0.9 pad_maximum_fusion
  1.7 1.5 select_convert_fusion
  3.2 1.5 copy.19.rope_key
  4.7 201.2 %shard_map.154 = bf16[96,2048]{1,0:T(8,128)(2,1)} custom-call(bf16[384,512]{1,0:T(8,128)(2,1)} %q_latent.1, bf16[384,256]{1,0:T(8,128)(2,1)} %kv_latent.1, bf16[384,64]{1,0:T(8,128)(2,1)} %copy.19.rope_key, f32[384,64]{1,0:T(8,128)} %get-tuple-element.10.cos_ref, f32[384,64]{1,0:T(8,128)} %get-tuple-element.11.sin_ref, ...), custom_call_target="tpu_custom_call" | custom-call | tf_op jit(solution)/shard_map/pallas_call | solution.py:855
  205.9 1.8 copy.21
  (2 shorter events, 0.0 us)
where the time goes:
time: 209 us; the launch traced here: 208 us
  Pallas kernels  201 us (96%)
  local copies, waits for them, and re-layouts  3.3 us (2%)
  other arithmetic  3.19 us (2%)
    pallas_call x1, Pallas kernels, fused_layer(): pl.pallas_call(functools.partial(layer_kernel, nz, ny, heads), out_shape=...  201 us

commit v1 on v0

--- a/solution.py
+++ b/solution.py
@@ -306,11 +306,9 @@
     heads,
     q_latent,
     kv_latent,
-    rope_key,
+    side_ref,
     cos_ref,
     sin_ref,
-    q_side,
-    k_side,
     q_gain,
     kv_gain,
     mix_gain,
@@ -326,7 +324,6 @@
     out_ref,
     packed,
     queries,
-    keys,
     vals,
     scores,
     top_ref,
@@ -442,17 +439,16 @@
         one.start()
 
     kv_normed = rms_rows(kv_latent[...], kv_gain[...])
-    cos_t, sin_t = cos_ref[...], sin_ref[...]
+    cos_t = jnp.concatenate([cos_ref[...], cos_ref[...]], axis=1)
+    sin_t = jnp.concatenate([-sin_ref[...], sin_ref[...]], axis=1)
 
     def turn(values):
         swapped = jnp.concatenate([values[:, RD // 2 :], values[:, : RD // 2]], axis=1)
         return values * cos_t + swapped * sin_t
 
-    key_rot = turn(rope_key[...].astype(jnp.float32))
-    tail_lanes = jnp.concatenate([key_rot, k_side[...].astype(jnp.float32)], axis=1)
     own_at = pl.multiple_of(sp * tok, tok)
     packed[pl.ds(own_at, tok), :rank] = kv_normed
-    packed[pl.ds(own_at, tok), rank:] = tail_lanes.astype(jnp.bfloat16)
+    packed[pl.ds(own_at, tok), rank:] = side_ref[...]
 
     barrier = pltpu.get_barrier_semaphore()
     mates = z_mates + [y_mate, x_mate, c_mate, diagonal]
@@ -473,19 +469,16 @@
     for s in range(1, nz):
         begin(remote(own_half, own_half, kvz_s.at[s - 1], kvz_r.at[s - 1], z_mates[s - 1]))
     begin(remote(own_half, own_half, kvy_s.at[0], kvy_r.at[0], y_mate))
-    for s in range(1, nz):
-        slots = weight_slots(sp)
-        for m, src in enumerate(weight_sources((z + s) % nz)):
-            begin(remote(src, slots[m], wz_s.at[s - 1, m], wz_r.at[s - 1, m], z_mates[s - 1]))
-
     q_normed = rms_rows(q_latent[...], q_gain[...])
+    own_mark = side_ref[...].astype(jnp.float32)[:, RD:]
+    q_side = jnp.where(own_mark > 0.5, 0.0, -1e30)
     for h in range(heads):
         wide_q = jnp.dot(
             q_normed,
             w_query[:, h * (NOPE + RD) : (h + 1) * (NOPE + RD)],
             preferred_element_type=jnp.float32,
         )
-        rest = jnp.concatenate([turn(wide_q[:, NOPE:]), q_side[...].astype(jnp.float32)], axis=1)
+        rest = jnp.concatenate([turn(wide_q[:, NOPE:]), q_side], axis=1)
         queries[h, :, :NOPE] = wide_q[:, :NOPE].astype(jnp.bfloat16)
         queries[h, :, NOPE:] = rest.astype(jnp.bfloat16)
 
@@ -501,6 +494,10 @@
         begin(remote(block, block, kvy_s.at[s], kvy_r.at[s], y_mate))
         begin(remote(block, block, kvc_s.at[s - 1], kvc_r.at[s - 1], c_mate))
     slots = weight_slots(sp)
+    for m in range(3):
+        for s in range(1, nz):
+            src = weight_sources((z + s) % nz)[m]
+            begin(remote(src, slots[m], wz_s.at[s - 1, m], wz_r.at[s - 1, m], z_mates[s - 1]))
     for m in range(3):
         local[m].wait()
         begin(remote(slots[m], slots[m], wy_s.at[0, m], wy_r.at[0, m], y_mate))
@@ -515,79 +512,90 @@
         block = half_of(source_y(s), 1 - c)
         remote(block, block, kvc_s.at[nz - 1 + s], kvc_r.at[nz - 1 + s], c_mate).wait_recv()
 
-    chunk = scores.shape[2]
+    chunk = scores.shape[3]
     chunks = total // chunk
     scale = (NOPE + RD) ** (-0.5) * log2_e
 
-    def one_head(h, carry):
-        top_ref[...] = jnp.full_like(top_ref, -3.0e38)
-        head_lanes = pl.ds(pl.multiple_of(h * NOPE, NOPE), NOPE)
-
-        def score_chunk(k, inner):
-            rows = pl.ds(pl.multiple_of(k * chunk, chunk), chunk)
-            latent = packed[rows, :rank]
-            keys[:, :NOPE] = jnp.dot(
-                latent, w_key[:, head_lanes], preferred_element_type=jnp.float32
-            ).astype(jnp.bfloat16)
-            vals[rows, :] = jnp.dot(
-                latent, w_value[:, head_lanes], preferred_element_type=jnp.float32
-            ).astype(jnp.bfloat16)
-            keys[:, NOPE:] = packed[rows, rank:]
-            value = lax.dot_general(
-                queries[h], keys[...], (((1,), (1,)), ((), ())), preferred_element_type=jnp.float32
-            )
-            scores[k] = value
-            most = top_ref[...]
-            for j in range(chunk // LANES):
-                most = jnp.maximum(most, value[:, j * LANES : (j + 1) * LANES])
-            top_ref[...] = most
-            return inner
-
-        lax.fori_loop(0, chunks, score_chunk, 0)
-        top = jnp.max(top_ref[...], axis=1, keepdims=True)
-        den_ref[...] = jnp.zeros_like(den_ref)
-        acc_ref[...] = jnp.zeros_like(acc_ref)
-
-        def weigh_chunk(k, inner):
-            rows = pl.ds(pl.multiple_of(k * chunk, chunk), chunk)
-            weights = jnp.exp2((scores[k] - top) * scale)
-            denom = den_ref[...]
-            for j in range(chunk // LANES):
-                denom = denom + weights[:, j * LANES : (j + 1) * LANES]
-            den_ref[...] = denom
-            acc_ref[...] += jnp.dot(
-                weights.astype(jnp.bfloat16), vals[rows, :], preferred_element_type=jnp.float32
-            )
-            return inner
-
-        lax.fori_loop(0, chunks, weigh_chunk, 0)
-        denom = jnp.sum(den_ref[...], axis=1, keepdims=True)
-        attended[:, head_lanes] = (acc_ref[...] / denom).astype(jnp.bfloat16)
-        return carry
-
-    lax.fori_loop(0, heads, one_head, 0)
-
-    def rows_of(peer):
-        return attended.at[pl.ds(pl.multiple_of(peer * quarter, quarter), quarter), :]
-
-    my_slot = head_rows.at[tp]
-    tp_mates = [(1, c_mate), (2, x_mate), (3, diagonal)]
+    def pass_weights(m):
+        for s in range(1, nz):
+            got = weight_slots(source(s))[m]
+            remote(got, got, wz_s.at[s - 1, m], wz_r.at[s - 1, m], z_mates[s - 1]).wait_recv()
+            begin(remote(got, got, wy_s.at[s, m], wy_r.at[s, m], y_mate))
+
+    def score_chunk(h, k):
+        rows = pl.ds(pl.multiple_of(k * chunk, chunk), chunk)
+        lanes = slice(h * NOPE, (h + 1) * NOPE)
+        both = jnp.dot(
+            packed[rows, :rank],
+            jnp.concatenate([w_key[:, lanes], w_value[:, lanes]], axis=1),
+            preferred_element_type=jnp.float32,
+        ).astype(jnp.bfloat16)
+        vals[h % 2, rows, :] = both[:, NOPE:]
+        keys = jnp.concatenate([both[:, :NOPE], packed[rows, rank:]], axis=1)
+        value = lax.dot_general(
+            queries[h], keys, (((1,), (1,)), ((), ())), preferred_element_type=jnp.float32
+        )
+        scores[h % 2, k] = value
+        most = top_ref[...]
+        for j in range(chunk // LANES):
+            most = jnp.maximum(most, value[:, j * LANES : (j + 1) * LANES])
+        top_ref[...] = most
+
+    def weigh_chunk(h, k, top):
+        rows = pl.ds(pl.multiple_of(k * chunk, chunk), chunk)
+        weights = jnp.exp2((scores[h % 2, k] - top) * scale)
+        denom = den_ref[...]
+        for j in range(chunk // LANES):
+            denom = denom + weights[:, j * LANES : (j + 1) * LANES]
+        den_ref[...] = denom
+        acc_ref[...] += jnp.dot(
+            weights.astype(jnp.bfloat16), vals[h % 2, rows, :], preferred_element_type=jnp.float32
+        )
+
+    tp_mates = [c_mate, x_mate, diagonal]
     tp_of = [x * CORES + 1 - c, (1 - x) * CORES + c, (1 - x) * CORES + 1 - c]
-    for i in (2, 1, 0):
-        begin(remote(rows_of(tp_of[i]), my_slot, tp_s.at[i], tp_r.at[i], tp_mates[i][1]))
+
+    def head_piece(h, i):
+        lanes = slice(h * VD, (h + 1) * VD)
+        rows = pl.ds(pl.multiple_of(tp_of[i] * quarter, quarter), quarter)
+        return remote(
+            attended.at[rows, lanes], head_rows.at[tp, :, lanes], tp_s.at[i, h], tp_r.at[i, h], tp_mates[i]
+        )
+
+    def head_arrives(h, i):
+        slot = head_rows.at[tp_of[i], :, slice(h * VD, (h + 1) * VD)]
+        remote(slot, slot, tp_s.at[i, h], tp_r.at[i, h], tp_mates[i]).wait_recv()
+
+    for h in range(heads + 1):
+        top = None
+        if h > 0:
+            top = jnp.max(top_ref[...], axis=1, keepdims=True)
+            den_ref[...] = jnp.zeros_like(den_ref)
+            acc_ref[...] = jnp.zeros_like(acc_ref)
+        if h < heads:
+            top_ref[...] = jnp.full_like(top_ref, -3.0e38)
+
+        def one_chunk(k, carry, h=h, top=top):
+            if h > 0:
+                weigh_chunk(h - 1, k, top)
+            if h < heads:
+                score_chunk(h, k)
+            return carry
+
+        lax.fori_loop(0, chunks, one_chunk, 0)
+        if h > 0:
+            denom = jnp.sum(den_ref[...], axis=1, keepdims=True)
+            attended[:, (h - 1) * VD : h * VD] = (acc_ref[...] / denom).astype(jnp.bfloat16)
+            for i in (2, 1, 0):
+                begin(head_piece(h - 1, i))
+
     head_rows[tp] = attended[pl.ds(pl.multiple_of(tp * quarter, quarter), quarter), :]
-
-    def pass_weights(s):
-        got = weight_slots(source(s))
-        for m in range(3):
-            remote(got[m], got[m], wz_s.at[s - 1, m], wz_r.at[s - 1, m], z_mates[s - 1]).wait_recv()
-            begin(remote(got[m], got[m], wy_s.at[s, m], wy_r.at[s, m], y_mate))
-
-    pass_weights(1)
+    pass_weights(0)
     local[3].wait()
     local[4].wait()
-    for i in range(3):
-        remote(rows_of(tp_of[i]), head_rows.at[tp_of[i]], tp_s.at[i], tp_r.at[i], tp_mates[i][1]).wait_recv()
+    for h in range(heads):
+        for i in range(3):
+            head_arrives(h, i)
     span = head_rows.shape[2]
     mixed = resid_alpha * own_resid[...].astype(jnp.float32)
     for t in range(tp_count):
@@ -596,7 +604,6 @@
         )
     rows_all[z, x, c] = layer_scaled(mixed, mix_gain[...]).astype(jnp.bfloat16)
 
-    delay = 1
     first = piece_start(z)
     stale = z * wide - first
 
@@ -651,10 +658,13 @@
         x_send(zz).start()
         c_send(zz, x).start()
 
-    def mix_step(step):
+    def across_step(step):
         zz = near_order(step, z, nz)
         arrive_x(zz)
         c_send(zz, 1 - x).start()
+
+    def mix_step(step):
+        zz = near_order(nz - 1 - step, z, nz)
         arrive_c(zz, x)
         arrive_c(zz, 1 - x)
         rows = 2 * CORES * quarter
@@ -682,7 +692,7 @@
         return pair_sum(zz, x) + x_part[zz].astype(jnp.float32)
 
     def chain_step(step):
-        above = step - z - 1
+        above = nz - 1 - step + z
 
         @pl.when(jnp.logical_and(above > z, above < nz))
         def _():
@@ -698,7 +708,7 @@
             up_sum_send(above).start()
 
         mirrored = nz - 1 - z
-        below_m = step - mirrored - 1
+        below_m = nz - 1 - step + mirrored
         below = nz - 1 - below_m
 
         @pl.when(jnp.logical_and(below_m > mirrored, below_m < nz))
@@ -715,20 +725,23 @@
             dn_sum_send(below).start()
 
     gather_step(jnp.int32(0))
-    for s in range(2, nz):
-        pass_weights(s)
-    for s in range(nz):
-        got = weight_slots(source_y(s))
-        for m in range(3):
-            remote(got[m], got[m], wy_s.at[s, m], wy_r.at[s, m], y_mate).wait_recv()
+    for step in range(1, nz):
+        if step < 3:
+            pass_weights(step)
+        gather_step(jnp.int32(step))
+        across_step(jnp.int32(step - 1))
+    across_step(jnp.int32(nz - 1))
+    for m in range(3):
+        for s in range(nz):
+            got = weight_slots(source_y(s))[m]
+            remote(got, got, wy_s.at[s, m], wy_r.at[s, m], y_mate).wait_recv()
 
     def one_step(step, carry):
-        pl.when(step < nz)(lambda: gather_step(step))
-        pl.when(step <= nz)(lambda: mix_step(step - 1))
-        chain_step(step - delay)
+        mix_step(step)
+        pl.when(step > 0)(lambda: chain_step(step - 1))
         return carry
 
-    lax.fori_loop(1, 2 * nz - 1 + delay, one_step, 0)
+    lax.fori_loop(0, nz, one_step, 0)
 
     ffn_sum = ready_sum(z)
     pl.when(z > 0)(up_sum_send(z).wait_recv)
@@ -790,11 +803,9 @@
     chunk = 512
     positions = lax.axis_index("sp") * tok + jnp.arange(tok, dtype=jnp.int32)
     cos_table, sin_table = rope_angles(positions)
-    cos_wide = jnp.concatenate([cos_table, cos_table], axis=1)
-    sin_wide = jnp.concatenate([-sin_table, sin_table], axis=1)
-    marks = (doc_ids[:, None] == jnp.arange(RD, dtype=jnp.int32)[None, :])
-    k_side = jnp.where(marks, 1.0, 0.0).astype(jnp.bfloat16)
-    q_side = jnp.where(marks, 0.0, -1e30).astype(jnp.bfloat16)
+    key_rot = rotate(rope_key.astype(jnp.float32), cos_table, sin_table).astype(jnp.bfloat16)
+    marks = doc_ids[:, None] == jnp.arange(RD, dtype=jnp.int32)[None, :]
+    side = jnp.concatenate([key_rot, marks.astype(jnp.bfloat16)], axis=1)
     vmem = pl.BlockSpec(memory_space=pltpu.VMEM)
     hbm = pl.BlockSpec(memory_space=pl.ANY)
     bf16, f32 = jnp.bfloat16, jnp.float32
@@ -802,9 +813,8 @@
     scratch = [
         pltpu.VMEM((total, rank + 2 * RD), bf16),
         pltpu.VMEM((heads, tok, NOPE + 2 * RD), bf16),
-        pltpu.VMEM((chunk, NOPE + 2 * RD), bf16),
-        pltpu.VMEM((total, VD), bf16),
-        pltpu.VMEM((total // chunk, tok, chunk), f32),
+        pltpu.VMEM((2, total, VD), bf16),
+        pltpu.VMEM((2, total // chunk, tok, chunk), f32),
         pltpu.VMEM((tok, LANES), f32),
         pltpu.VMEM((tok, LANES), f32),
         pltpu.VMEM((tok, VD), f32),
@@ -835,8 +845,8 @@
         dma((nz - 1, 3)),
         dma((nz, 3)),
         dma((nz, 3)),
-        dma((3,)),
-        dma((3,)),
+        dma((3, heads)),
+        dma((3, heads)),
         dma((nz,)),
         dma((nz,)),
         dma((nz,)),
@@ -855,7 +865,7 @@
     return pl.pallas_call(
         functools.partial(layer_kernel, nz, ny, heads),
         out_shape=jax.ShapeDtypeStruct((quarter, model), bf16),
-        in_specs=[vmem] * 14 + [hbm] * 5,
+        in_specs=[vmem] * 12 + [hbm] * 5,
         out_specs=vmem,
         scratch_shapes=scratch,
         compiler_params=pltpu.CompilerParams(
@@ -864,11 +874,9 @@
     )(
         q_latent,
         kv_latent,
-        rope_key,
-        cos_wide,
-        sin_wide,
-        q_side,
-        k_side,
+        side,
+        cos_table,
+        sin_table,
         q_gain[None, :],
         kv_gain[None, :],
         mix_gain[None, :],

time: 209 us -> 157 us (0.75)
  Pallas kernels: 201 us -> 149 us
    pallas_call x1, Pallas kernels: 201 us -> 149 us  [fused_layer(): pl.pallas_call(functools.partial(layer_kernel, nz, ny, heads), out_shape=...]
where the time goes in v1:
time: 157 us; the launch traced here: 155 us
  Pallas kernels  149 us (95%)
  other arithmetic  3.16 us (2%)
  local copies, waits for them, and re-layouts  2.68 us (2%)
    pallas_call x1, Pallas kernels, fused_layer(): pl.pallas_call(functools.partial(layer_kernel, nz, ny, heads), out_shape=...  149 us

profile of v1, /device:TPU:16, one launch (start us, length us, event | category | flops | bytes accessed | tf_op | source)
XLA Modules:
  0.0 155.1 jit_solution(16695810566508604698)
XLA Ops:
  0.0 0.9 copy.18
  1.0 1.6 %subtract_convert_fusion = (bf16[384,32]{1,0:T(8,128)(2,1)S(1)}, bf16[384,32]{1,0:T(8,128)(2,1)S(1)}, f32[384,32]{1,0:T(8,128)}, f32[384,32]{1,0:T(8,128)}) fusion(f32[384,64]{1,0:T(8,128)S(1)} %convert_element_type.14, f32[384]{0:T(512)S(1)} %add_convert_fusion.1, f32[32]{0:T(128)S(1)} %multiply_power_fusion), kind=kLoop, calls=%fused_computation.4 | loop fusion | flops 110592 | bytes 247424 | tf_op jit(solution)/shard_map/convert
  2.5 0.8 fusion
  3.3 0.8 pad_maximum_fusion.side_ref
  4.1 149.2 %shard_map.154 = bf16[96,2048]{1,0:T(8,128)(2,1)} custom-call(bf16[384,512]{1,0:T(8,128)(2,1)} %q_latent.1, bf16[384,256]{1,0:T(8,128)(2,1)} %kv_latent.1, bf16[384,128]{1,0:T(8,128)(2,1)} %pad_maximum_fusion.side_ref, f32[384,32]{1,0:T(8,128)} %get-tuple-element.8.cos_ref, f32[384,32]{1,0:T(8,128)} %get-tuple-element.7.sin_ref, f32[1,512]{1,0:T(1,128)} %bitcast.6, ...), custom_call_target="tpu_custom_call" | custom-call | tf_op jit(solution)/shard_map/pallas_call | solution.py:865
  153.3 1.8 %copy.21 = bf16[96,2048]{1,0:T(8,128)(2,1)} copy(bf16[96,2048]{1,0:T(8,128)(2,1)} %shard_map.154) | data formatting | bytes 786432
  (3 shorter events, 0.0 us)

commit v2 on v1

--- a/solution.py
+++ b/solution.py
@@ -3,6 +3,7 @@
 
 import jax
 import jax.numpy as jnp
+import numpy as np
 from jax import lax
 from jax.experimental import pallas as pl
 from jax.experimental.pallas import tpu as pltpu
@@ -300,15 +301,41 @@
     return jnp.where(step <= paired, close, wide)
 
 
+def turn_table(total):
+    steps = np.arange(0, RD, 2, dtype=np.float32) / np.float32(RD)
+    frequency = np.power(np.float32(rope_theta), -steps, dtype=np.float32)
+    angles = frequency[:, None] * np.arange(total, dtype=np.float32)[None, :]
+    wide_angles = angles.astype(np.float64)
+    return np.concatenate([np.cos(wide_angles), np.sin(wide_angles)], axis=0).astype(np.float32)
+
+
 def layer_kernel(
     nz,
     ny,
     heads,
     q_latent,
     kv_latent,
-    side_ref,
-    cos_ref,
-    sin_ref,
+    rope_turned,
+    doc_row,
+    table,
+    q_gain_in,
+    kv_gain_in,
+    mix_gain_in,
+    out_gain_in,
+    w_query_in,
+    w_key_in,
+    w_value_in,
+    resid,
+    w_out,
+    w_gate,
+    w_up,
+    w_down,
+    out_ref,
+    q_lat,
+    kv_lat,
+    rope_own,
+    doc_own,
+    turns,
     q_gain,
     kv_gain,
     mix_gain,
@@ -316,12 +343,6 @@
     w_query,
     w_key,
     w_value,
-    resid,
-    w_out,
-    w_gate,
-    w_up,
-    w_down,
-    out_ref,
     packed,
     queries,
     vals,
@@ -343,13 +364,19 @@
     x_stage,
     x_part,
     z_stage,
-    up_part,
-    dn_part,
+    z_part,
+    late_stage,
+    late_part,
+    last_stage,
+    last_part,
     loc_sem,
+    own_sem,
     kvz_s,
     kvz_r,
     kvy_s,
     kvy_r,
+    kvx_s,
+    kvx_r,
     kvc_s,
     kvc_r,
     wz_s,
@@ -370,15 +397,16 @@
     xrs_s,
     xrs_r,
     zch_s,
-    zup_r,
-    zdn_r,
+    zch_r,
+    late_s,
+    late_r,
+    last_sem,
 ):
     sp = lax.axis_index("sp")
     tp = lax.axis_index("tp")
     z, y = sp // ny, sp % ny
     x, c = tp // CORES, tp % CORES
     tok = q_latent.shape[0]
-    half = tok // CORES
     quarter = out_ref.shape[0]
     tp_count = tok // quarter
     depth = w_gate.shape[0]
@@ -411,49 +439,100 @@
     diagonal = at(xx=1 - x, cc=1 - c)
     z_mates = [at(zz=(z + s) % nz) for s in range(1, nz)]
 
-    def piece_start(zz):
-        return pl.multiple_of(jnp.minimum(zz * wide, ff - wide), LANES)
-
-    def weight_slots(src_sp):
-        rows = pl.ds(pl.multiple_of(src_sp * depth, depth), depth)
-        return (gate_w.at[rows, :], up_w.at[rows, :], down_w.at[:, rows])
-
-    def weight_sources(zz):
-        lanes = pl.ds(piece_start(zz), wide)
-        rows = pl.ds(piece_start(zz), wide)
-        return (w_gate.at[:, lanes], w_up.at[:, lanes], w_down.at[rows, :])
-
-    local = [
-        pltpu.make_async_copy(src, dst, loc_sem.at[i])
-        for i, (src, dst) in enumerate(zip(weight_sources(z), weight_slots(sp)))
-    ]
-    local.append(pltpu.make_async_copy(w_out, out_weights, loc_sem.at[3]))
-    local.append(
-        pltpu.make_async_copy(
-            resid.at[pl.ds(pl.multiple_of(tp * quarter, quarter), quarter), :],
-            own_resid,
-            loc_sem.at[4],
-        )
-    )
-    for one in local:
-        one.start()
-
-    kv_normed = rms_rows(kv_latent[...], kv_gain[...])
-    cos_t = jnp.concatenate([cos_ref[...], cos_ref[...]], axis=1)
-    sin_t = jnp.concatenate([-sin_ref[...], sin_ref[...]], axis=1)
-
-    def turn(values):
-        swapped = jnp.concatenate([values[:, RD // 2 :], values[:, : RD // 2]], axis=1)
-        return values * cos_t + swapped * sin_t
-
-    own_at = pl.multiple_of(sp * tok, tok)
-    packed[pl.ds(own_at, tok), :rank] = kv_normed
-    packed[pl.ds(own_at, tok), rank:] = side_ref[...]
-
     barrier = pltpu.get_barrier_semaphore()
     mates = z_mates + [y_mate, x_mate, c_mate, diagonal]
     for mate in mates:
         pl.semaphore_signal(barrier, inc=1, device_id=mate, device_id_type=MESH)
+
+    tiles = wide // LANES
+    missing = nz * tiles - ff // LANES
+
+    def is_short(zz):
+        return (zz + nz - (nz // 2 - 1 + c)) % nz < missing
+
+    def piece_start(zz):
+        begun = 0
+        for other in range(nz - 1):
+            begun = begun + jnp.where(other < zz, tiles - is_short(other).astype(jnp.int32), 0)
+        return pl.multiple_of(begun * LANES, LANES)
+
+    def by_width(zz, make):
+        pairs = [(jnp.logical_not(is_short(zz)), make(wide))]
+        if missing:
+            pairs.append((is_short(zz), make(wide - LANES)))
+        return pairs
+
+    def when_start(pairs):
+        for wanted, copy in pairs:
+            pl.when(wanted)(copy.start)
+
+    def when_wait_recv(pairs):
+        for wanted, copy in pairs:
+            pl.when(wanted)(copy.wait_recv)
+
+    def weight_slot(src_sp, m, width):
+        rows = pl.ds(pl.multiple_of(src_sp * depth, depth), depth)
+        if m == 2:
+            return down_w.at[pl.ds(0, width), rows]
+        return (gate_w, up_w)[m].at[rows, pl.ds(0, width)]
+
+    def weight_source(zz, m, width):
+        units = pl.ds(piece_start(zz), width)
+        return w_down.at[units, :] if m == 2 else (w_gate, w_up)[m].at[:, units]
+
+    def own_weights(m):
+        return by_width(
+            z,
+            lambda width: pltpu.make_async_copy(
+                weight_source(z, m, width), weight_slot(sp, m, width), own_sem.at[m]
+            ),
+        )
+
+    own_cols = pl.ds(pl.multiple_of(sp * tok, LANES), tok)
+    own_quarter = pl.ds(pl.multiple_of(tp * quarter, quarter), quarter)
+    moves = [
+        (kv_latent, kv_lat),
+        (kv_gain_in, kv_gain),
+        (rope_turned, rope_own),
+        (doc_row, doc_own),
+        (table.at[:, own_cols], turns),
+        (q_latent, q_lat),
+        (q_gain_in, q_gain),
+        (w_query_in, w_query),
+        (w_key_in, w_key),
+        (w_value_in, w_value),
+        (mix_gain_in, mix_gain),
+        (out_gain_in, out_gain),
+        (resid.at[own_quarter, :], own_resid),
+        (w_out, out_weights),
+    ]
+    local = [pltpu.make_async_copy(src, dst, loc_sem.at[n]) for n, (src, dst) in enumerate(moves)]
+    for one in local:
+        one.start()
+    for m in range(3):
+        when_start(own_weights(m))
+    if missing:
+
+        @pl.when(is_short(z))
+        def _():
+            down_w[wide - LANES :, :] = jnp.zeros((LANES, model), jnp.bfloat16)
+
+    for n in range(5):
+        local[n].wait()
+    half_turn = RD // 2
+    cos_rows = jnp.concatenate([turns[:half_turn], turns[:half_turn]], axis=0)
+    sin_rows = jnp.concatenate([-turns[half_turn:], turns[half_turn:]], axis=0)
+    rope = rope_own[...].astype(jnp.float32)
+    flipped = jnp.concatenate([rope[half_turn:], rope[:half_turn]], axis=0)
+    marks = lax.broadcasted_iota(jnp.int32, (RD, tok), 0) == doc_own[...]
+    side_rows = jnp.concatenate(
+        [rope * cos_rows + flipped * sin_rows, marks.astype(jnp.float32)], axis=0
+    )
+    side = side_rows.T
+    own_at = pl.multiple_of(sp * tok, tok)
+    packed[pl.ds(own_at, tok), :rank] = rms_rows(kv_lat[...], kv_gain[...])
+    packed[pl.ds(own_at, tok), rank:] = side.astype(jnp.bfloat16)
+
     pl.semaphore_wait(barrier, len(mates))
 
     sends = []
@@ -462,55 +541,98 @@
         copy.start()
         sends.append(copy)
 
-    def half_of(src_sp, cc):
-        return packed.at[pl.ds(pl.multiple_of(src_sp * tok + cc * half, half), half), :]
-
-    own_half = half_of(sp, c)
+    def latent_piece(src_sp, xx, cc):
+        first_row = src_sp * tok + (xx * CORES + cc) * quarter
+        return packed.at[pl.ds(pl.multiple_of(first_row, quarter), quarter), :]
+
+    def source(s):
+        return ((z + nz - s) % nz) * ny + y
+
+    def source_y(s):
+        return ((z + nz - s) % nz) * ny + (1 - y)
+
+    foreign = [source(s) for s in range(1, nz)] + [source_y(s) for s in range(nz)]
+    own_piece = latent_piece(sp, x, c)
     for s in range(1, nz):
-        begin(remote(own_half, own_half, kvz_s.at[s - 1], kvz_r.at[s - 1], z_mates[s - 1]))
-    begin(remote(own_half, own_half, kvy_s.at[0], kvy_r.at[0], y_mate))
-    q_normed = rms_rows(q_latent[...], q_gain[...])
-    own_mark = side_ref[...].astype(jnp.float32)[:, RD:]
-    q_side = jnp.where(own_mark > 0.5, 0.0, -1e30)
+        begin(remote(own_piece, own_piece, kvz_s.at[s - 1], kvz_r.at[s - 1], z_mates[s - 1]))
+    begin(remote(own_piece, own_piece, kvy_s.at[0], kvy_r.at[0], y_mate))
+
+    for n in range(5, 8):
+        local[n].wait()
+    both_turns = jnp.concatenate([cos_rows, sin_rows], axis=0).T
+    cos_t, sin_t = both_turns[:, :RD], both_turns[:, RD:]
+    q_normed = rms_rows(q_lat[...], q_gain[...])
+    q_side = jnp.where(side[:, RD:] > 0.5, 0.0, -1e30)
     for h in range(heads):
         wide_q = jnp.dot(
             q_normed,
             w_query[:, h * (NOPE + RD) : (h + 1) * (NOPE + RD)],
             preferred_element_type=jnp.float32,
         )
-        rest = jnp.concatenate([turn(wide_q[:, NOPE:]), q_side], axis=1)
+        turned = wide_q[:, NOPE:]
+        swapped = jnp.concatenate([turned[:, half_turn:], turned[:, :half_turn]], axis=1)
+        rest = jnp.concatenate([turned * cos_t + swapped * sin_t, q_side], axis=1)
         queries[h, :, :NOPE] = wide_q[:, :NOPE].astype(jnp.bfloat16)
         queries[h, :, NOPE:] = rest.astype(jnp.bfloat16)
 
-    def source(s):
-        return ((z + nz - s) % nz) * ny + y
-
-    def source_y(s):
-        return ((z + nz - s) % nz) * ny + (1 - y)
+    def hand_on(n):
+        piece = latent_piece(foreign[n], x, c)
+        begin(remote(piece, piece, kvx_s.at[n], kvx_r.at[n], x_mate))
+        begin(remote(piece, piece, kvc_s.at[0, n], kvc_r.at[0, n], c_mate))
 
     for s in range(1, nz):
-        block = half_of(source(s), c)
-        remote(block, block, kvz_s.at[s - 1], kvz_r.at[s - 1], z_mates[s - 1]).wait_recv()
-        begin(remote(block, block, kvy_s.at[s], kvy_r.at[s], y_mate))
-        begin(remote(block, block, kvc_s.at[s - 1], kvc_r.at[s - 1], c_mate))
-    slots = weight_slots(sp)
+        piece = latent_piece(source(s), x, c)
+        remote(piece, piece, kvz_s.at[s - 1], kvz_r.at[s - 1], z_mates[s - 1]).wait_recv()
+        begin(remote(piece, piece, kvy_s.at[s], kvy_r.at[s], y_mate))
+        hand_on(s - 1)
+
+    def weight_z(s, m):
+        return by_width(
+            (z + s) % nz,
+            lambda width: remote(
+                weight_source((z + s) % nz, m, width),
+                weight_slot(sp, m, width),
+                wz_s.at[s - 1, m],
+                wz_r.at[s - 1, m],
+                z_mates[s - 1],
+            ),
+        )
+
+    def weight_z_in(s, m):
+        def make(width):
+            slot = weight_slot(source(s), m, width)
+            return remote(slot, slot, wz_s.at[s - 1, m], wz_r.at[s - 1, m], z_mates[s - 1])
+
+        return by_width(z, make)
+
+    def weight_y(s, m, src_sp):
+        def make(width):
+            slot = weight_slot(src_sp, m, width)
+            return remote(slot, slot, wy_s.at[s, m], wy_r.at[s, m], y_mate)
+
+        return by_width(z, make)
+
     for m in range(3):
         for s in range(1, nz):
-            src = weight_sources((z + s) % nz)[m]
-            begin(remote(src, slots[m], wz_s.at[s - 1, m], wz_r.at[s - 1, m], z_mates[s - 1]))
+            when_start(weight_z(s, m))
+    for s in range(nz):
+        piece = latent_piece(source_y(s), x, c)
+        remote(piece, piece, kvy_s.at[s], kvy_r.at[s], y_mate).wait_recv()
+        hand_on(nz - 1 + s)
     for m in range(3):
-        local[m].wait()
-        begin(remote(slots[m], slots[m], wy_s.at[0, m], wy_r.at[0, m], y_mate))
-    for s in range(nz):
-        block = half_of(source_y(s), c)
-        remote(block, block, kvy_s.at[s], kvy_r.at[s], y_mate).wait_recv()
-        begin(remote(block, block, kvc_s.at[nz - 1 + s], kvc_r.at[nz - 1 + s], c_mate))
-    for s in range(1, nz):
-        block = half_of(source(s), 1 - c)
-        remote(block, block, kvc_s.at[s - 1], kvc_r.at[s - 1], c_mate).wait_recv()
-    for s in range(nz):
-        block = half_of(source_y(s), 1 - c)
-        remote(block, block, kvc_s.at[nz - 1 + s], kvc_r.at[nz - 1 + s], c_mate).wait_recv()
+        for wanted, copy in own_weights(m):
+            pl.when(wanted)(copy.wait)
+        when_start(weight_y(0, m, sp))
+    for n, src_sp in enumerate(foreign):
+        piece = latent_piece(src_sp, 1 - x, c)
+        remote(piece, piece, kvx_s.at[n], kvx_r.at[n], x_mate).wait_recv()
+        begin(remote(piece, piece, kvc_s.at[1, n], kvc_r.at[1, n], c_mate))
+    for n, src_sp in enumerate(foreign):
+        for k, xx in enumerate((x, 1 - x)):
+            piece = latent_piece(src_sp, xx, 1 - c)
+            remote(piece, piece, kvc_s.at[k, n], kvc_r.at[k, n], c_mate).wait_recv()
+    local[8].wait()
+    local[9].wait()
 
     chunk = scores.shape[3]
     chunks = total // chunk
@@ -518,9 +640,8 @@
 
     def pass_weights(m):
         for s in range(1, nz):
-            got = weight_slots(source(s))[m]
-            remote(got, got, wz_s.at[s - 1, m], wz_r.at[s - 1, m], z_mates[s - 1]).wait_recv()
-            begin(remote(got, got, wy_s.at[s, m], wy_r.at[s, m], y_mate))
+            when_wait_recv(weight_z_in(s, m))
+            when_start(weight_y(s, m, source(s)))
 
     def score_chunk(h, k):
         rows = pl.ds(pl.multiple_of(k * chunk, chunk), chunk)
@@ -589,10 +710,10 @@
             for i in (2, 1, 0):
                 begin(head_piece(h - 1, i))
 
+    pass_weights(0)
     head_rows[tp] = attended[pl.ds(pl.multiple_of(tp * quarter, quarter), quarter), :]
-    pass_weights(0)
-    local[3].wait()
-    local[4].wait()
+    for n in range(10, len(local)):
+        local[n].wait()
     for h in range(heads):
         for i in range(3):
             head_arrives(h, i)
@@ -604,125 +725,182 @@
         )
     rows_all[z, x, c] = layer_scaled(mixed, mix_gain[...]).astype(jnp.bfloat16)
 
-    first = piece_start(z)
-    stale = z * wide - first
-
-    def z_sends(zz):
-        block = rows_all.at[zz, x, c]
+    kept = jnp.where(is_short(z), wide - LANES, wide) if missing else wide
+
+    halves = [slice(0, model // 2), slice(model // 2, model)]
+
+    def z_sends(zz, n):
+        block = rows_all.at[zz, x, c, :, halves[n]]
+        arrives = z_r.at[zz, n]
         return (
-            (jnp.logical_and(zz <= z, z < nz - 1), remote(block, block, up_s.at[zz], z_r.at[zz], at(zz=jnp.minimum(z + 1, nz - 1)))),
-            (jnp.logical_and(zz >= z, z > 0), remote(block, block, dn_s.at[zz], z_r.at[zz], at(zz=jnp.maximum(z - 1, 0)))),
-        )
-
-    def x_send(zz):
-        block = rows_all.at[zz, x, c]
-        return remote(block, block, x_s.at[zz], x_r.at[zz], x_mate)
-
-    def c_send(zz, xx):
-        block = rows_all.at[zz, xx, c]
-        return remote(block, block, c_s.at[zz, xx], c_r.at[zz, xx], c_mate)
-
-    def arrive_x(zz):
-        block = rows_all.at[zz, 1 - x, c]
-        remote(block, block, x_s.at[zz], x_r.at[zz], x_mate).wait_recv()
-
-    def arrive_c(zz, xx):
-        block = rows_all.at[zz, xx, 1 - c]
-        remote(block, block, c_s.at[zz, xx], c_r.at[zz, xx], c_mate).wait_recv()
+            (
+                jnp.logical_and(zz <= z, z < nz - 1),
+                remote(block, block, up_s.at[zz, n], arrives, at(zz=jnp.minimum(z + 1, nz - 1))),
+            ),
+            (
+                jnp.logical_and(zz >= z, z > 0),
+                remote(block, block, dn_s.at[zz, n], arrives, at(zz=jnp.maximum(z - 1, 0))),
+            ),
+        )
+
+    def x_send(zz, n):
+        block = rows_all.at[zz, x, c, :, halves[n]]
+        return remote(block, block, x_s.at[zz, n], x_r.at[zz, n], x_mate)
+
+    def c_send(zz, xx, n):
+        block = rows_all.at[zz, xx, c, :, halves[n]]
+        return remote(block, block, c_s.at[zz, xx, n], c_r.at[zz, xx, n], c_mate)
+
+    def arrive_x(zz, n):
+        block = rows_all.at[zz, 1 - x, c, :, halves[n]]
+        remote(block, block, x_s.at[zz, n], x_r.at[zz, n], x_mate).wait_recv()
+
+    def arrive_c(zz, xx, n):
+        block = rows_all.at[zz, xx, 1 - c, :, halves[n]]
+        remote(block, block, c_s.at[zz, xx, n], c_r.at[zz, xx, n], c_mate).wait_recv()
+
+    bend = x_stage.shape[2]
 
     def core_send(zz, xx):
-        return remote(part.at[zz, xx, 1 - c], core_part.at[zz, xx], crs_s.at[zz, xx], crs_r.at[zz, xx], c_mate)
-
-    def x_sum_send(zz):
-        return remote(x_stage.at[zz], x_part.at[zz], xrs_s.at[zz], xrs_r.at[zz], x_mate)
-
-    def up_sum_send(zz):
-        return remote(z_stage.at[zz], up_part.at[zz], zch_s.at[zz], zup_r.at[zz], at(zz=jnp.minimum(z + 1, nz - 1)))
-
-    def dn_sum_send(zz):
-        return remote(z_stage.at[zz], dn_part.at[zz], zch_s.at[zz], zdn_r.at[zz], at(zz=jnp.maximum(z - 1, 0)))
-
-    def pair_sum(zz, xx):
-        return part[zz, xx, c].astype(jnp.float32) + core_part[zz, xx].astype(jnp.float32)
+        return remote(
+            part.at[zz, xx, 1 - c], core_part.at[zz, xx], crs_s.at[zz, xx], crs_r.at[zz, xx], c_mate
+        )
+
+    middle = -(-bend // (2 * LANES)) * LANES
+    cuts = [slice(0, middle), slice(middle, bend)]
+
+    def x_sum_send(zz, n):
+        cols = cuts[n]
+        return remote(
+            x_stage.at[zz, :, cols], x_part.at[zz, :, cols], xrs_s.at[zz, n], xrs_r.at[zz, n], x_mate
+        )
+
+    def last_send():
+        return remote(last_stage, last_part, last_sem.at[0], last_sem.at[1], x_mate)
+
+    def beyond(way):
+        return at(zz=jnp.clip(jnp.where(way == 0, z + 1, z - 1), 0, nz - 1))
+
+    def sum_send(zz, n, way):
+        cols = cuts[n]
+        return remote(
+            z_stage.at[zz, :, cols],
+            z_part.at[way, zz, :, cols],
+            zch_s.at[zz, n],
+            zch_r.at[way, zz, n],
+            beyond(way),
+        )
+
+    def late_send(zz, way):
+        return remote(
+            late_stage.at[zz], late_part.at[way, zz], late_s.at[zz], late_r.at[way, zz], beyond(way)
+        )
+
+    def pair_sum(zz, xx, cols):
+        return part[zz, xx, c, :, cols].astype(jnp.float32) + core_part[zz, xx, :, cols].astype(
+            jnp.float32
+        )
+
+    late_cols = slice(bend, model)
 
     def gather_step(step):
         zz = near_order(step, z, nz)
-
-        @pl.when(step > 0)
-        def _():
-            block = rows_all.at[zz, x, c]
-            remote(block, block, up_s.at[zz], z_r.at[zz], x_mate).wait_recv()
-
-        for wanted, copy in z_sends(zz):
-            pl.when(wanted)(copy.start)
-        x_send(zz).start()
-        c_send(zz, x).start()
+        for n in range(2):
+
+            @pl.when(step > 0)
+            def _(n=n):
+                block = rows_all.at[zz, x, c, :, halves[n]]
+                remote(block, block, up_s.at[zz, n], z_r.at[zz, n], x_mate).wait_recv()
+
+            for wanted, copy in z_sends(zz, n):
+                pl.when(wanted)(copy.start)
+            x_send(zz, n).start()
+            c_send(zz, x, n).start()
 
     def across_step(step):
         zz = near_order(step, z, nz)
-        arrive_x(zz)
-        c_send(zz, 1 - x).start()
+        for n in range(2):
+            arrive_x(zz, n)
+            c_send(zz, 1 - x, n).start()
 
     def mix_step(step):
-        zz = near_order(nz - 1 - step, z, nz)
-        arrive_c(zz, x)
-        arrive_c(zz, 1 - x)
-        rows = 2 * CORES * quarter
+        zz = near_order(jnp.where(step == 0, 0, nz - step), z, nz)
+        for n in range(2):
+            arrive_c(zz, x, n)
+            arrive_c(zz, 1 - x, n)
+        rows = CORES * quarter
         lanes = lax.broadcasted_iota(jnp.int32, (1, wide), 1)
-        unit = rows_all[zz].reshape(rows, model)
-        gate = jnp.dot(unit, gate_w[...], preferred_element_type=jnp.float32)
-        up = jnp.dot(unit, up_w[...], preferred_element_type=jnp.float32)
-        inner = jax.nn.silu(gate) * up
-        hidden[...] = jnp.where(lanes >= stale, inner, 0.0).astype(jnp.bfloat16)
-        cut = 512
-        for n in range(model // cut):
-            piece = jnp.dot(
-                hidden[...], down_w[:, n * cut : (n + 1) * cut], preferred_element_type=jnp.float32
-            ).astype(jnp.bfloat16)
-            part[zz, :, :, :, n * cut : (n + 1) * cut] = piece.reshape(2, CORES, quarter, cut)
-        core_send(zz, 1 - x).start()
-        core_send(zz, x).start()
+        for xx in (1 - x, x):
+            unit = rows_all[zz, xx].reshape(rows, model)
+            gate = jnp.dot(unit, gate_w[...], preferred_element_type=jnp.float32)
+            up = jnp.dot(unit, up_w[...], preferred_element_type=jnp.float32)
+            inner = jax.nn.silu(gate) * up
+            hidden[...] = jnp.where(lanes < kept, inner, 0.0).astype(jnp.bfloat16)
+            cut = 512
+            for n in range(model // cut):
+                piece = jnp.dot(
+                    hidden[...], down_w[:, n * cut : (n + 1) * cut], preferred_element_type=jnp.float32
+                ).astype(jnp.bfloat16)
+                part[zz, xx, :, :, n * cut : (n + 1) * cut] = piece.reshape(CORES, quarter, cut)
+            core_send(zz, xx).start()
         core_send(zz, 1 - x).wait_recv()
-        x_stage[zz] = pair_sum(zz, 1 - x).astype(jnp.bfloat16)
-        x_sum_send(zz).start()
-
-    def ready_sum(zz):
-        core_send(zz, x).wait_recv()
-        x_sum_send(zz).wait_recv()
-        return pair_sum(zz, x) + x_part[zz].astype(jnp.float32)
+        for n in range(2):
+            x_stage[zz, :, cuts[n]] = pair_sum(zz, 1 - x, cuts[n]).astype(jnp.bfloat16)
+            x_sum_send(zz, n).start()
+
+    def ready_sum(zz, n):
+        x_sum_send(zz, n).wait_recv()
+        return pair_sum(zz, x, cuts[n]) + x_part[zz, :, cuts[n]].astype(jnp.float32)
+
+    def handed_on(step):
+        for turn in range(2):
+            way = jnp.where(z < nz // 2, 1 - turn, turn)
+            place = jnp.where(way == 0, z, nz - 1 - z)
+            owner = nz - 1 - step + place
+            wanted = jnp.logical_and(owner > place, owner < nz)
+            yield way, jnp.where(way == 0, owner, nz - 1 - owner), wanted, place > 0
 
     def chain_step(step):
-        above = nz - 1 - step + z
-
-        @pl.when(jnp.logical_and(above > z, above < nz))
-        def _():
-            z_stage[above] = ready_sum(above).astype(jnp.bfloat16)
-
-            @pl.when(z > 0)
-            def _():
-                up_sum_send(above).wait_recv()
-                z_stage[above] = (
-                    z_stage[above].astype(jnp.float32) + up_part[above].astype(jnp.float32)
-                ).astype(jnp.bfloat16)
-
-            up_sum_send(above).start()
-
-        mirrored = nz - 1 - z
-        below_m = nz - 1 - step + mirrored
-        below = nz - 1 - below_m
-
-        @pl.when(jnp.logical_and(below_m > mirrored, below_m < nz))
-        def _():
-            z_stage[below] = ready_sum(below).astype(jnp.bfloat16)
-
-            @pl.when(mirrored > 0)
-            def _():
-                dn_sum_send(below).wait_recv()
-                z_stage[below] = (
-                    z_stage[below].astype(jnp.float32) + dn_part[below].astype(jnp.float32)
-                ).astype(jnp.bfloat16)
-
-            dn_sum_send(below).start()
+        for way, zz, wanted, relayed in handed_on(step):
+
+            @pl.when(wanted)
+            def _(way=way, zz=zz, relayed=relayed):
+                for n in range(2):
+                    cols = cuts[n]
+                    z_stage[zz, :, cols] = ready_sum(zz, n).astype(jnp.bfloat16)
+
+                    @pl.when(relayed)
+                    def _(n=n, cols=cols):
+                        sum_send(zz, n, way).wait_recv()
+                        z_stage[zz, :, cols] = (
+                            z_stage[zz, :, cols].astype(jnp.float32)
+                            + z_part[way, zz, :, cols].astype(jnp.float32)
+                        ).astype(jnp.bfloat16)
+
+                    sum_send(zz, n, way).start()
+
+    def late_step(step):
+        for way, zz, wanted, relayed in handed_on(step):
+
+            @pl.when(wanted)
+            def _(way=way, zz=zz, relayed=relayed):
+                core_send(zz, x).wait_recv()
+                for xx in range(2):
+                    late_stage[zz, xx] = pair_sum(zz, xx, late_cols).astype(jnp.bfloat16)
+
+                @pl.when(relayed)
+                def _():
+                    late_send(zz, way).wait_recv()
+                    late_stage[zz] = (
+                        late_stage[zz].astype(jnp.float32) + late_part[way, zz].astype(jnp.float32)
+                    ).astype(jnp.bfloat16)
+
+                late_send(zz, way).start()
+
+    def late_total(xx):
+        got = pair_sum(z, xx, late_cols)
+        got = got + jnp.where(z > 0, late_part[0, z, xx].astype(jnp.float32), 0.0)
+        return got + jnp.where(z < nz - 1, late_part[1, z, xx].astype(jnp.float32), 0.0)
 
     gather_step(jnp.int32(0))
     for step in range(1, nz):
@@ -730,41 +908,65 @@
             pass_weights(step)
         gather_step(jnp.int32(step))
         across_step(jnp.int32(step - 1))
-    across_step(jnp.int32(nz - 1))
     for m in range(3):
         for s in range(nz):
-            got = weight_slots(source_y(s))[m]
-            remote(got, got, wy_s.at[s, m], wy_r.at[s, m], y_mate).wait_recv()
+            when_wait_recv(weight_y(s, m, source_y(s)))
 
     def one_step(step, carry):
         mix_step(step)
-        pl.when(step > 0)(lambda: chain_step(step - 1))
+        pl.when(step == 0)(lambda: across_step(nz - 1))
+        pl.when(step > 0)(lambda: late_step(step - 1))
+        pl.when(step > 1)(lambda: chain_step(step - 2))
         return carry
 
     lax.fori_loop(0, nz, one_step, 0)
-
-    ffn_sum = ready_sum(z)
-    pl.when(z > 0)(up_sum_send(z).wait_recv)
-    pl.when(z < nz - 1)(dn_sum_send(z).wait_recv)
-    part_sum = ffn_sum + jnp.where(z > 0, up_part[z].astype(jnp.float32), 0.0)
-    part_sum = part_sum + jnp.where(z < nz - 1, dn_part[z].astype(jnp.float32), 0.0)
+    core_send(z, x).wait_recv()
+    pl.when(z > 0)(late_send(z, 0).wait_recv)
+    pl.when(z < nz - 1)(late_send(z, 1).wait_recv)
+    last_stage[...] = late_total(1 - x).astype(jnp.bfloat16)
+    last_send().start()
+    late_sum = late_total(x)
+    chain_step(nz - 2)
+
+    totals = []
+    for n in range(2):
+        cols = cuts[n]
+        got = ready_sum(z, n)
+        pl.when(z > 0)(sum_send(z, n, 0).wait_recv)
+        pl.when(z < nz - 1)(sum_send(z, n, 1).wait_recv)
+        got = got + jnp.where(z > 0, z_part[0, z, :, cols].astype(jnp.float32), 0.0)
+        totals.append(got + jnp.where(z < nz - 1, z_part[1, z, :, cols].astype(jnp.float32), 0.0))
+    last_send().wait_recv()
+    late_sum = late_sum + last_part[...].astype(jnp.float32)
+    part_sum = jnp.concatenate(totals + [late_sum], axis=1)
     out_ref[...] = layer_scaled(
         resid_alpha * rows_all[z, x, c].astype(jnp.float32) + 0.5 * part_sum, out_gain[...]
     ).astype(jnp.bfloat16)
 
     for copy in sends:
         copy.wait_send()
+    for m in range(3):
+        pairs = weight_y(0, m, sp)
+        for s in range(1, nz):
+            pairs = pairs + weight_z(s, m) + weight_y(s, m, source(s))
+        for wanted, copy in pairs:
+            pl.when(wanted)(copy.wait_send)
+
+    last_send().wait_send()
 
     def drain(zz, carry):
-        for wanted, copy in z_sends(zz):
-            pl.when(wanted)(copy.wait_send)
-        x_send(zz).wait_send()
+        for n in range(2):
+            for wanted, copy in z_sends(zz, n):
+                pl.when(wanted)(copy.wait_send)
+            x_send(zz, n).wait_send()
+            for xx in range(2):
+                c_send(zz, xx, n).wait_send()
         for xx in range(2):
-            c_send(zz, xx).wait_send()
             core_send(zz, xx).wait_send()
-        x_sum_send(zz).wait_send()
-        pl.when(zz > z)(up_sum_send(zz).wait_send)
-        pl.when(zz < z)(dn_sum_send(zz).wait_send)
+        for n in range(2):
+            x_sum_send(zz, n).wait_send()
+            pl.when(zz != z)(sum_send(zz, n, 0).wait_send)
+        pl.when(zz != z)(late_send(zz, 0).wait_send)
         return carry
 
     lax.fori_loop(0, nz, drain, 0)
@@ -801,16 +1003,25 @@
     ff = w_gate.shape[1]
     wide = -(-ff // (LANES * nz)) * LANES
     chunk = 512
-    positions = lax.axis_index("sp") * tok + jnp.arange(tok, dtype=jnp.int32)
-    cos_table, sin_table = rope_angles(positions)
-    key_rot = rotate(rope_key.astype(jnp.float32), cos_table, sin_table).astype(jnp.bfloat16)
-    marks = doc_ids[:, None] == jnp.arange(RD, dtype=jnp.int32)[None, :]
-    side = jnp.concatenate([key_rot, marks.astype(jnp.bfloat16)], axis=1)
+    bend = model - 3 * (model // 16)
     vmem = pl.BlockSpec(memory_space=pltpu.VMEM)
     hbm = pl.BlockSpec(memory_space=pl.ANY)
     bf16, f32 = jnp.bfloat16, jnp.float32
     dma = pltpu.SemaphoreType.DMA
+    table = turn_table(total)
     scratch = [
+        pltpu.VMEM(q_latent.shape, bf16),
+        pltpu.VMEM(kv_latent.shape, bf16),
+        pltpu.VMEM((RD, tok), bf16),
+        pltpu.VMEM((1, tok), jnp.int32),
+        pltpu.VMEM((RD, tok), f32),
+        pltpu.VMEM((1, q_latent.shape[1]), f32),
+        pltpu.VMEM((1, rank), f32),
+        pltpu.VMEM((1, model), f32),
+        pltpu.VMEM((1, model), f32),
+        pltpu.VMEM(w_query.shape, bf16),
+        pltpu.VMEM(w_key.shape, bf16),
+        pltpu.VMEM(w_value.shape, bf16),
         pltpu.VMEM((total, rank + 2 * RD), bf16),
         pltpu.VMEM((heads, tok, NOPE + 2 * RD), bf16),
         pltpu.VMEM((2, total, VD), bf16),
@@ -826,46 +1037,54 @@
         pltpu.VMEM((model, wide), bf16),
         pltpu.VMEM((wide, model), bf16),
         pltpu.VMEM((nz, 2, CORES, quarter, model), bf16),
-        pltpu.VMEM((2 * CORES * quarter, wide), bf16),
+        pltpu.VMEM((CORES * quarter, wide), bf16),
         pltpu.VMEM((nz, 2, CORES, quarter, model), bf16),
         pltpu.VMEM((nz, 2, quarter, model), bf16),
-        pltpu.VMEM((nz, quarter, model), bf16),
-        pltpu.VMEM((nz, quarter, model), bf16),
-        pltpu.VMEM((nz, quarter, model), bf16),
-        pltpu.VMEM((nz, quarter, model), bf16),
-        pltpu.VMEM((nz, quarter, model), bf16),
-        dma((5,)),
+        pltpu.VMEM((nz, quarter, bend), bf16),
+        pltpu.VMEM((nz, quarter, bend), bf16),
+        pltpu.VMEM((nz, quarter, bend), bf16),
+        pltpu.VMEM((2, nz, quarter, bend), bf16),
+        pltpu.VMEM((nz, 2, quarter, model - bend), bf16),
+        pltpu.VMEM((2, nz, 2, quarter, model - bend), bf16),
+        pltpu.VMEM((quarter, model - bend), bf16),
+        pltpu.VMEM((quarter, model - bend), bf16),
+        dma((14,)),
+        dma((3,)),
         dma((nz - 1,)),
         dma((nz - 1,)),
         dma((nz,)),
         dma((nz,)),
         dma((2 * nz - 1,)),
         dma((2 * nz - 1,)),
+        dma((2, 2 * nz - 1)),
+        dma((2, 2 * nz - 1)),
         dma((nz - 1, 3)),
         dma((nz - 1, 3)),
         dma((nz, 3)),
         dma((nz, 3)),
         dma((3, heads)),
         dma((3, heads)),
-        dma((nz,)),
-        dma((nz,)),
-        dma((nz,)),
-        dma((nz,)),
-        dma((nz,)),
         dma((nz, 2)),
         dma((nz, 2)),
         dma((nz, 2)),
         dma((nz, 2)),
+        dma((nz, 2)),
+        dma((nz, 2, 2)),
+        dma((nz, 2, 2)),
+        dma((nz, 2)),
+        dma((nz, 2)),
+        dma((nz, 2)),
+        dma((nz, 2)),
+        dma((nz, 2)),
+        dma((2, nz, 2)),
         dma((nz,)),
-        dma((nz,)),
-        dma((nz,)),
-        dma((nz,)),
-        dma((nz,)),
+        dma((2, nz)),
+        dma((2,)),
     ]
     return pl.pallas_call(
         functools.partial(layer_kernel, nz, ny, heads),
         out_shape=jax.ShapeDtypeStruct((quarter, model), bf16),
-        in_specs=[vmem] * 12 + [hbm] * 5,
+        in_specs=[hbm] * 17,
         out_specs=vmem,
         scratch_shapes=scratch,
         compiler_params=pltpu.CompilerParams(
@@ -874,9 +1093,9 @@
     )(
         q_latent,
         kv_latent,
-        side,
-        cos_table,
-        sin_table,
+        rope_key.T,
+        doc_ids[None, :],
+        table,
         q_gain[None, :],
         kv_gain[None, :],
         mix_gain[None, :],

time: 157 us -> 133 us (0.85)
  Pallas kernels: 149 us -> 129 us
  other arithmetic: 3.16 us -> 0 us
    pallas_call x1, Pallas kernels: 149 us -> 129 us  [fused_layer(): pl.pallas_call(functools.partial(layer_kernel, nz, ny, heads), out_shape=...]
    another operation x1 -> x0, other arithmetic: 1.57 us -> none
where the time goes in v2:
time: 133 us; the launch traced here: 132 us
  Pallas kernels  129 us (97%)
  local copies, waits for them, and re-layouts  3.01 us (2%)
    pallas_call x1, Pallas kernels, fused_layer(): pl.pallas_call(functools.partial(layer_kernel, nz, ny, heads), out_shape=...  129 us

profile of v2, /device:TPU:16, one launch (start us, length us, event | category | flops | bytes accessed | tf_op | source)
XLA Modules:
  0.0 132.5 jit_solution(17987632664416655743)
XLA Ops:
  0.0 1.2 broadcast_in_dim.15.doc_row
  1.2 129.5 %shard_map.163 = bf16[96,2048]{1,0:T(8,128)(2,1)} custom-call(bf16[384,512]{1,0:T(8,128)(2,1)} %q_latent.1, bf16[384,256]{1,0:T(8,128)(2,1)} %kv_latent.1, bf16[64,384]{1,0:T(8,128)(2,1)} %bitcast.5, s32[1,384]{1,0:T(1,128)} %broadcast_in_dim.15.doc_row, f32[64,3072]{1,0:T(8,128)} %constant.2.clone.table, f32[1,512]{1,0:T(1,128)} %bitcast.8, ...), custom_call_target="tpu_custom_call" | custom-call | tf_op jit(solution)/shard_map/pallas_call | solution.py:1084
  130.7 1.8 %copy.19 = bf16[96,2048]{1,0:T(8,128)(2,1)} copy(bf16[96,2048]{1,0:T(8,128)(2,1)} %shard_map.163) | data formatting | bytes 786432

commit v3 on v2

--- a/solution.py
+++ b/solution.py
@@ -524,7 +524,7 @@
     sin_rows = jnp.concatenate([-turns[half_turn:], turns[half_turn:]], axis=0)
     rope = rope_own[...].astype(jnp.float32)
     flipped = jnp.concatenate([rope[half_turn:], rope[:half_turn]], axis=0)
-    marks = lax.broadcasted_iota(jnp.int32, (RD, tok), 0) == doc_own[...]
+    marks = lax.broadcasted_iota(jnp.int32, (RD, tok), 0) == doc_own[...][None, :]
     side_rows = jnp.concatenate(
         [rope * cos_rows + flipped * sin_rows, marks.astype(jnp.float32)], axis=0
     )
@@ -535,11 +535,8 @@
 
     pl.semaphore_wait(barrier, len(mates))
 
-    sends = []
-
     def begin(copy):
         copy.start()
-        sends.append(copy)
 
     def latent_piece(src_sp, xx, cc):
         first_row = src_sp * tok + (xx * CORES + cc) * quarter
@@ -554,7 +551,7 @@
     foreign = [source(s) for s in range(1, nz)] + [source_y(s) for s in range(nz)]
     own_piece = latent_piece(sp, x, c)
     for s in range(1, nz):
-        begin(remote(own_piece, own_piece, kvz_s.at[s - 1], kvz_r.at[s - 1], z_mates[s - 1]))
+        begin(remote(own_piece, own_piece, kvz_s.at[0], kvz_r.at[s - 1], z_mates[s - 1]))
     begin(remote(own_piece, own_piece, kvy_s.at[0], kvy_r.at[0], y_mate))
 
     for n in range(5, 8):
@@ -577,13 +574,13 @@
 
     def hand_on(n):
         piece = latent_piece(foreign[n], x, c)
-        begin(remote(piece, piece, kvx_s.at[n], kvx_r.at[n], x_mate))
-        begin(remote(piece, piece, kvc_s.at[0, n], kvc_r.at[0, n], c_mate))
+        begin(remote(piece, piece, kvx_s.at[0], kvx_r.at[n], x_mate))
+        begin(remote(piece, piece, kvc_s.at[0], kvc_r.at[0], c_mate))
 
     for s in range(1, nz):
         piece = latent_piece(source(s), x, c)
-        remote(piece, piece, kvz_s.at[s - 1], kvz_r.at[s - 1], z_mates[s - 1]).wait_recv()
-        begin(remote(piece, piece, kvy_s.at[s], kvy_r.at[s], y_mate))
+        remote(piece, piece, kvz_s.at[0], kvz_r.at[s - 1], z_mates[s - 1]).wait_recv()
+        begin(remote(piece, piece, kvy_s.at[0], kvy_r.at[s], y_mate))
         hand_on(s - 1)
 
     def weight_z(s, m):
@@ -605,10 +602,21 @@
 
         return by_width(z, make)
 
-    def weight_y(s, m, src_sp):
+    def weight_y(m, src_sp):
         def make(width):
             slot = weight_slot(src_sp, m, width)
-            return remote(slot, slot, wy_s.at[s, m], wy_r.at[s, m], y_mate)
+            return remote(slot, slot, wy_s.at[m], wy_r.at[m], y_mate)
+
+        return by_width(z, make)
+
+    def weight_y_all(m):
+        def make(width):
+            rows = pl.ds(0, nz * depth)
+            if m == 2:
+                slot = down_w.at[pl.ds(0, width), rows]
+            else:
+                slot = (gate_w, up_w)[m].at[rows, pl.ds(0, width)]
+            return remote(slot, slot, wy_s.at[m], wy_r.at[m], y_mate)
 
         return by_width(z, make)
 
@@ -617,20 +625,22 @@
             when_start(weight_z(s, m))
     for s in range(nz):
         piece = latent_piece(source_y(s), x, c)
-        remote(piece, piece, kvy_s.at[s], kvy_r.at[s], y_mate).wait_recv()
+        remote(piece, piece, kvy_s.at[0], kvy_r.at[s], y_mate).wait_recv()
         hand_on(nz - 1 + s)
     for m in range(3):
         for wanted, copy in own_weights(m):
             pl.when(wanted)(copy.wait)
-        when_start(weight_y(0, m, sp))
+        when_start(weight_y(m, sp))
     for n, src_sp in enumerate(foreign):
         piece = latent_piece(src_sp, 1 - x, c)
-        remote(piece, piece, kvx_s.at[n], kvx_r.at[n], x_mate).wait_recv()
-        begin(remote(piece, piece, kvc_s.at[1, n], kvc_r.at[1, n], c_mate))
-    for n, src_sp in enumerate(foreign):
-        for k, xx in enumerate((x, 1 - x)):
-            piece = latent_piece(src_sp, xx, 1 - c)
-            remote(piece, piece, kvc_s.at[k, n], kvc_r.at[k, n], c_mate).wait_recv()
+        remote(piece, piece, kvx_s.at[0], kvx_r.at[n], x_mate).wait_recv()
+        begin(remote(piece, piece, kvc_s.at[0], kvc_r.at[0], c_mate))
+
+    def latent_bytes(count, send, recv):
+        rows = packed.at[pl.ds(0, count * quarter), :]
+        return remote(rows, rows, send, recv, c_mate)
+
+    latent_bytes(2 * len(foreign), kvc_s.at[0], kvc_r.at[0]).wait_recv()
     local[8].wait()
     local[9].wait()
 
@@ -641,7 +651,7 @@
     def pass_weights(m):
         for s in range(1, nz):
             when_wait_recv(weight_z_in(s, m))
-            when_start(weight_y(s, m, source(s)))
+            when_start(weight_y(m, source(s)))
 
     def score_chunk(h, k):
         rows = pl.ds(pl.multiple_of(k * chunk, chunk), chunk)
@@ -680,12 +690,17 @@
         lanes = slice(h * VD, (h + 1) * VD)
         rows = pl.ds(pl.multiple_of(tp_of[i] * quarter, quarter), quarter)
         return remote(
-            attended.at[rows, lanes], head_rows.at[tp, :, lanes], tp_s.at[i, h], tp_r.at[i, h], tp_mates[i]
-        )
-
-    def head_arrives(h, i):
-        slot = head_rows.at[tp_of[i], :, slice(h * VD, (h + 1) * VD)]
-        remote(slot, slot, tp_s.at[i, h], tp_r.at[i, h], tp_mates[i]).wait_recv()
+            attended.at[rows, lanes], head_rows.at[tp, :, lanes], tp_s.at[0], tp_r.at[0], tp_mates[i]
+        )
+
+    def heads_all():
+        return remote(
+            attended.at[pl.ds(0, tok - quarter), :],
+            head_rows.at[pl.ds(0, tp_count - 1)],
+            tp_s.at[0],
+            tp_r.at[0],
+            c_mate,
+        )
 
     for h in range(heads + 1):
         top = None
@@ -714,9 +729,7 @@
     head_rows[tp] = attended[pl.ds(pl.multiple_of(tp * quarter, quarter), quarter), :]
     for n in range(10, len(local)):
         local[n].wait()
-    for h in range(heads):
-        for i in range(3):
-            head_arrives(h, i)
+    heads_all().wait_recv()
     span = head_rows.shape[2]
     mixed = resid_alpha * own_resid[...].astype(jnp.float32)
     for t in range(tp_count):
@@ -727,7 +740,8 @@
 
     kept = jnp.where(is_short(z), wide - LANES, wide) if missing else wide
 
-    halves = [slice(0, model // 2), slice(model // 2, model)]
+    pieces = z_r.shape[1]
+    halves = [slice(n * model // pieces, (n + 1) * model // pieces) for n in range(pieces)]
 
     def z_sends(zz, n):
         block = rows_all.at[zz, x, c, :, halves[n]]
@@ -735,35 +749,35 @@
         return (
             (
                 jnp.logical_and(zz <= z, z < nz - 1),
-                remote(block, block, up_s.at[zz, n], arrives, at(zz=jnp.minimum(z + 1, nz - 1))),
+                remote(block, block, up_s.at[zz], arrives, at(zz=jnp.minimum(z + 1, nz - 1))),
             ),
             (
                 jnp.logical_and(zz >= z, z > 0),
-                remote(block, block, dn_s.at[zz, n], arrives, at(zz=jnp.maximum(z - 1, 0))),
+                remote(block, block, dn_s.at[zz], arrives, at(zz=jnp.maximum(z - 1, 0))),
             ),
         )
 
     def x_send(zz, n):
         block = rows_all.at[zz, x, c, :, halves[n]]
-        return remote(block, block, x_s.at[zz, n], x_r.at[zz, n], x_mate)
+        return remote(block, block, x_s.at[0], x_r.at[zz, n], x_mate)
 
     def c_send(zz, xx, n):
         block = rows_all.at[zz, xx, c, :, halves[n]]
-        return remote(block, block, c_s.at[zz, xx, n], c_r.at[zz, xx, n], c_mate)
+        return remote(block, block, c_s.at[0], c_r.at[zz, xx], c_mate)
 
     def arrive_x(zz, n):
         block = rows_all.at[zz, 1 - x, c, :, halves[n]]
-        remote(block, block, x_s.at[zz, n], x_r.at[zz, n], x_mate).wait_recv()
-
-    def arrive_c(zz, xx, n):
-        block = rows_all.at[zz, xx, 1 - c, :, halves[n]]
-        remote(block, block, c_s.at[zz, xx, n], c_r.at[zz, xx, n], c_mate).wait_recv()
+        remote(block, block, x_s.at[0], x_r.at[zz, n], x_mate).wait_recv()
+
+    def arrive_c(zz, xx):
+        block = rows_all.at[zz, xx, 1 - c]
+        remote(block, block, c_s.at[0], c_r.at[zz, xx], c_mate).wait_recv()
 
     bend = x_stage.shape[2]
 
     def core_send(zz, xx):
         return remote(
-            part.at[zz, xx, 1 - c], core_part.at[zz, xx], crs_s.at[zz, xx], crs_r.at[zz, xx], c_mate
+            part.at[zz, xx, 1 - c], core_part.at[zz, xx], crs_s.at[0], crs_r.at[zz, xx], c_mate
         )
 
     middle = -(-bend // (2 * LANES)) * LANES
@@ -772,7 +786,7 @@
     def x_sum_send(zz, n):
         cols = cuts[n]
         return remote(
-            x_stage.at[zz, :, cols], x_part.at[zz, :, cols], xrs_s.at[zz, n], xrs_r.at[zz, n], x_mate
+            x_stage.at[zz, :, cols], x_part.at[zz, :, cols], xrs_s.at[0], xrs_r.at[zz, n], x_mate
         )
 
     def last_send():
@@ -786,14 +800,14 @@
         return remote(
             z_stage.at[zz, :, cols],
             z_part.at[way, zz, :, cols],
-            zch_s.at[zz, n],
+            zch_s.at[0],
             zch_r.at[way, zz, n],
             beyond(way),
         )
 
     def late_send(zz, way):
         return remote(
-            late_stage.at[zz], late_part.at[way, zz], late_s.at[zz], late_r.at[way, zz], beyond(way)
+            late_stage.at[zz], late_part.at[way, zz], late_s.at[0], late_r.at[way, zz], beyond(way)
         )
 
     def pair_sum(zz, xx, cols):
@@ -805,12 +819,12 @@
 
     def gather_step(step):
         zz = near_order(step, z, nz)
-        for n in range(2):
+        for n in range(pieces):
 
             @pl.when(step > 0)
             def _(n=n):
                 block = rows_all.at[zz, x, c, :, halves[n]]
-                remote(block, block, up_s.at[zz, n], z_r.at[zz, n], x_mate).wait_recv()
+                remote(block, block, up_s.at[zz], z_r.at[zz, n], x_mate).wait_recv()
 
             for wanted, copy in z_sends(zz, n):
                 pl.when(wanted)(copy.start)
@@ -819,30 +833,35 @@
 
     def across_step(step):
         zz = near_order(step, z, nz)
-        for n in range(2):
+        for n in range(pieces):
             arrive_x(zz, n)
             c_send(zz, 1 - x, n).start()
 
+    def mix_half(turn, step):
+        zz = near_order(jnp.where(step == 0, 0, nz - step), z, nz)
+        late_rows = step == 1
+        xx = jnp.where((turn == 0) == late_rows, x, 1 - x)
+        pl.when(jnp.logical_and(late_rows, turn == 1))(lambda: across_step(nz - 1))
+        arrive_c(zz, xx)
+        rows = CORES * quarter
+        lanes = lax.broadcasted_iota(jnp.int32, (1, wide), 1)
+        unit = rows_all[zz, xx].reshape(rows, model)
+        gate = jnp.dot(unit, gate_w[...], preferred_element_type=jnp.float32)
+        up = jnp.dot(unit, up_w[...], preferred_element_type=jnp.float32)
+        inner = jax.nn.silu(gate) * up
+        hidden[...] = jnp.where(lanes < kept, inner, 0.0).astype(jnp.bfloat16)
+        cut = 512
+        for n in range(model // cut):
+            piece = jnp.dot(
+                hidden[...], down_w[:, n * cut : (n + 1) * cut], preferred_element_type=jnp.float32
+            ).astype(jnp.bfloat16)
+            part[zz, xx, :, :, n * cut : (n + 1) * cut] = piece.reshape(CORES, quarter, cut)
+        core_send(zz, xx).start()
+        return step
+
     def mix_step(step):
         zz = near_order(jnp.where(step == 0, 0, nz - step), z, nz)
-        for n in range(2):
-            arrive_c(zz, x, n)
-            arrive_c(zz, 1 - x, n)
-        rows = CORES * quarter
-        lanes = lax.broadcasted_iota(jnp.int32, (1, wide), 1)
-        for xx in (1 - x, x):
-            unit = rows_all[zz, xx].reshape(rows, model)
-            gate = jnp.dot(unit, gate_w[...], preferred_element_type=jnp.float32)
-            up = jnp.dot(unit, up_w[...], preferred_element_type=jnp.float32)
-            inner = jax.nn.silu(gate) * up
-            hidden[...] = jnp.where(lanes < kept, inner, 0.0).astype(jnp.bfloat16)
-            cut = 512
-            for n in range(model // cut):
-                piece = jnp.dot(
-                    hidden[...], down_w[:, n * cut : (n + 1) * cut], preferred_element_type=jnp.float32
-                ).astype(jnp.bfloat16)
-                part[zz, xx, :, :, n * cut : (n + 1) * cut] = piece.reshape(CORES, quarter, cut)
-            core_send(zz, xx).start()
+        lax.fori_loop(0, 2, mix_half, step)
         core_send(zz, 1 - x).wait_recv()
         for n in range(2):
             x_stage[zz, :, cuts[n]] = pair_sum(zz, 1 - x, cuts[n]).astype(jnp.bfloat16)
@@ -909,12 +928,10 @@
         gather_step(jnp.int32(step))
         across_step(jnp.int32(step - 1))
     for m in range(3):
-        for s in range(nz):
-            when_wait_recv(weight_y(s, m, source_y(s)))
+        when_wait_recv(weight_y_all(m))
 
     def one_step(step, carry):
         mix_step(step)
-        pl.when(step == 0)(lambda: across_step(nz - 1))
         pl.when(step > 0)(lambda: late_step(step - 1))
         pl.when(step > 1)(lambda: chain_step(step - 2))
         return carry
@@ -943,30 +960,41 @@
         resid_alpha * rows_all[z, x, c].astype(jnp.float32) + 0.5 * part_sum, out_gain[...]
     ).astype(jnp.bfloat16)
 
-    for copy in sends:
-        copy.wait_send()
+    latent_bytes(nz - 1, kvz_s.at[0], kvz_r.at[0]).wait_send()
+    latent_bytes(nz, kvy_s.at[0], kvy_r.at[0]).wait_send()
+    latent_bytes(len(foreign), kvx_s.at[0], kvx_r.at[0]).wait_send()
+    latent_bytes(2 * len(foreign), kvc_s.at[0], kvc_r.at[0]).wait_send()
+    heads_all().wait_send()
     for m in range(3):
-        pairs = weight_y(0, m, sp)
+        pairs = weight_y_all(m)
         for s in range(1, nz):
-            pairs = pairs + weight_z(s, m) + weight_y(s, m, source(s))
+            pairs = pairs + weight_z(s, m)
         for wanted, copy in pairs:
             pl.when(wanted)(copy.wait_send)
 
     last_send().wait_send()
 
+    everywhere = rows_all.at[:, x, c]
+    remote(everywhere, everywhere, x_s.at[0], x_r.at[0, 0], x_mate).wait_send()
+    everywhere = rows_all.at[:, :, c]
+    remote(everywhere, everywhere, c_s.at[0], c_r.at[0, 0], c_mate).wait_send()
+    remote(part.at[:, :, 1 - c], core_part, crs_s.at[0], crs_r.at[0, 0], c_mate).wait_send()
+    remote(x_stage, x_part, xrs_s.at[0], xrs_r.at[0, 0], x_mate).wait_send()
+    others = pl.ds(0, nz - 1)
+    remote(
+        z_stage.at[others], z_part.at[0, others], zch_s.at[0], zch_r.at[0, 0, 0], x_mate
+    ).wait_send()
+    remote(
+        late_stage.at[others], late_part.at[0, others], late_s.at[0], late_r.at[0, 0], x_mate
+    ).wait_send()
+
     def drain(zz, carry):
-        for n in range(2):
-            for wanted, copy in z_sends(zz, n):
-                pl.when(wanted)(copy.wait_send)
-            x_send(zz, n).wait_send()
-            for xx in range(2):
-                c_send(zz, xx, n).wait_send()
-        for xx in range(2):
-            core_send(zz, xx).wait_send()
-        for n in range(2):
-            x_sum_send(zz, n).wait_send()
-            pl.when(zz != z)(sum_send(zz, n, 0).wait_send)
-        pl.when(zz != z)(late_send(zz, 0).wait_send)
+        block = rows_all.at[zz, x, c]
+        for wanted, sem in (
+            (jnp.logical_and(zz <= z, z < nz - 1), up_s),
+            (jnp.logical_and(zz >= z, z > 0), dn_s),
+        ):
+            pl.when(wanted)(remote(block, block, sem.at[zz], z_r.at[0, 0], x_mate).wait_send)
         return carry
 
     lax.fori_loop(0, nz, drain, 0)
@@ -1003,8 +1031,8 @@
     ff = w_gate.shape[1]
     wide = -(-ff // (LANES * nz)) * LANES
     chunk = 512
+    pieces = 4
     bend = model - 3 * (model // 16)
-    vmem = pl.BlockSpec(memory_space=pltpu.VMEM)
     hbm = pl.BlockSpec(memory_space=pl.ANY)
     bf16, f32 = jnp.bfloat16, jnp.float32
     dma = pltpu.SemaphoreType.DMA
@@ -1013,7 +1041,7 @@
         pltpu.VMEM(q_latent.shape, bf16),
         pltpu.VMEM(kv_latent.shape, bf16),
         pltpu.VMEM((RD, tok), bf16),
-        pltpu.VMEM((1, tok), jnp.int32),
+        pltpu.VMEM((tok,), jnp.int32),
         pltpu.VMEM((RD, tok), f32),
         pltpu.VMEM((1, q_latent.shape[1]), f32),
         pltpu.VMEM((1, rank), f32),
@@ -1050,51 +1078,51 @@
         pltpu.VMEM((quarter, model - bend), bf16),
         dma((14,)),
         dma((3,)),
+        dma((1,)),
         dma((nz - 1,)),
-        dma((nz - 1,)),
+        dma((1,)),
+        dma((nz,)),
+        dma((1,)),
+        dma((2 * nz - 1,)),
+        dma((1,)),
+        dma((1,)),
+        dma((nz - 1, 3)),
+        dma((nz - 1, 3)),
+        dma((3,)),
+        dma((3,)),
+        dma((1,)),
+        dma((1,)),
         dma((nz,)),
         dma((nz,)),
-        dma((2 * nz - 1,)),
-        dma((2 * nz - 1,)),
-        dma((2, 2 * nz - 1)),
-        dma((2, 2 * nz - 1)),
-        dma((nz - 1, 3)),
-        dma((nz - 1, 3)),
-        dma((nz, 3)),
-        dma((nz, 3)),
-        dma((3, heads)),
-        dma((3, heads)),
+        dma((nz, pieces)),
+        dma((1,)),
+        dma((nz, pieces)),
+        dma((1,)),
         dma((nz, 2)),
+        dma((1,)),
         dma((nz, 2)),
+        dma((1,)),
         dma((nz, 2)),
-        dma((nz, 2)),
-        dma((nz, 2)),
-        dma((nz, 2, 2)),
-        dma((nz, 2, 2)),
-        dma((nz, 2)),
-        dma((nz, 2)),
-        dma((nz, 2)),
-        dma((nz, 2)),
-        dma((nz, 2)),
+        dma((1,)),
         dma((2, nz, 2)),
-        dma((nz,)),
+        dma((1,)),
         dma((2, nz)),
         dma((2,)),
     ]
     return pl.pallas_call(
         functools.partial(layer_kernel, nz, ny, heads),
-        out_shape=jax.ShapeDtypeStruct((quarter, model), bf16),
+        out_shape=pltpu.VMEM((quarter, model), bf16),
         in_specs=[hbm] * 17,
-        out_specs=vmem,
+        out_specs=pl.BlockSpec(memory_space=pltpu.VMEM),
         scratch_shapes=scratch,
         compiler_params=pltpu.CompilerParams(
-            collective_id=0, has_side_effects=True, vmem_limit_bytes=67043328
+            collective_id=0, has_side_effects=True, vmem_limit_bytes=64 * 1000 * 1000
         ),
     )(
         q_latent,
         kv_latent,
         rope_key.T,
-        doc_ids[None, :],
+        doc_ids,
         table,
         q_gain[None, :],
         kv_gain[None, :],

time: 133 us -> 127 us (0.955)
  Pallas kernels: 129 us -> 126 us
  local copies, waits for them, and re-layouts: 3.01 us -> 0.75 us
    pallas_call x1, Pallas kernels: 129 us -> 126 us  [fused_layer(): pl.pallas_call(functools.partial(layer_kernel, nz, ny, heads), out_shape=...]
where the time goes in v3:
time: 127 us
  Pallas kernels  126 us (99%)
    pallas_call x1, Pallas kernels, fused_layer(): pl.pallas_call(functools.partial(layer_kernel, nz, ny, heads), out_shape=...  126 us

profile of v3, /device:TPU:16, one launch (start us, length us, event | category | flops | bytes accessed | tf_op | source)
XLA Modules:
  0.0 126.9 jit_solution(16267769137909379716)
XLA Ops:
  0.0 126.1 %shard_map.163 = bf16[96,2048]{1,0:T(8,128)(2,1)S(1)} custom-call(bf16[384,512]{1,0:T(8,128)(2,1)} %q_latent.1, bf16[384,256]{1,0:T(8,128)(2,1)} %kv_latent.1, bf16[64,384]{1,0:T(8,128)(2,1)} %bitcast.5, s32[384]{0:T(512)} %doc_row.1, f32[64,3072]{1,0:T(8,128)} %constant.2.clone.table, f32[1,512]{1,0:T(1,128)} %bitcast.8, f32[1,256]{1,0:T(1,128)} %bitcast.9, ...), custom_call_target="tpu_custom_call" | custom-call | tf_op jit(solution)/shard_map/pallas_call | solution.py:1112
  126.1 0.7 copy.19

commit v4 on v3

--- a/solution.py
+++ b/solution.py
@@ -725,7 +725,6 @@
             for i in (2, 1, 0):
                 begin(head_piece(h - 1, i))
 
-    pass_weights(0)
     head_rows[tp] = attended[pl.ds(pl.multiple_of(tp * quarter, quarter), quarter), :]
     for n in range(10, len(local)):
         local[n].wait()
@@ -859,13 +858,19 @@
         core_send(zz, xx).start()
         return step
 
+    inside = jnp.logical_and(z > 0, z < nz - 1)
+
+    def send_x_sum(zz, n):
+        x_stage[zz, :, cuts[n]] = pair_sum(zz, 1 - x, cuts[n]).astype(jnp.bfloat16)
+        x_sum_send(zz, n).start()
+
     def mix_step(step):
         zz = near_order(jnp.where(step == 0, 0, nz - step), z, nz)
         lax.fori_loop(0, 2, mix_half, step)
         core_send(zz, 1 - x).wait_recv()
-        for n in range(2):
-            x_stage[zz, :, cuts[n]] = pair_sum(zz, 1 - x, cuts[n]).astype(jnp.bfloat16)
-            x_sum_send(zz, n).start()
+        send_x_sum(zz, 0)
+        pl.when(jnp.logical_or(step > 0, inside))(lambda: send_x_sum(zz, 1))
+        pl.when(jnp.logical_and(step == nz - 1, jnp.logical_not(inside)))(lambda: send_x_sum(z, 1))
 
     def ready_sum(zz, n):
         x_sum_send(zz, n).wait_recv()
@@ -922,6 +927,7 @@
         return got + jnp.where(z < nz - 1, late_part[1, z, xx].astype(jnp.float32), 0.0)
 
     gather_step(jnp.int32(0))
+    pass_weights(0)
     for step in range(1, nz):
         if step < 3:
             pass_weights(step)
@@ -1030,9 +1036,9 @@
     rank = kv_latent.shape[1]
     ff = w_gate.shape[1]
     wide = -(-ff // (LANES * nz)) * LANES
-    chunk = 512
+    chunk = 1024
     pieces = 4
-    bend = model - 3 * (model // 16)
+    bend = model - model // 8
     hbm = pl.BlockSpec(memory_space=pl.ANY)
     bf16, f32 = jnp.bfloat16, jnp.float32
     dma = pltpu.SemaphoreType.DMA

time: 127 us -> 126 us (level)
  no operation moved by 1% of the time
where the time goes in v4:
time: 126 us
  Pallas kernels  126 us (100%)
    pallas_call x1, Pallas kernels, fused_layer(): pl.pallas_call(functools.partial(layer_kernel, nz, ny, heads), out_shape=...  126 us

profile of v4, /device:TPU:16, one launch (start us, length us, event | category | flops | bytes accessed | tf_op | source)
XLA Modules:
  0.0 126.3 jit_solution(2580198259065130897)
XLA Ops:
  0.0 125.6 %shard_map.163 = bf16[96,2048]{1,0:T(8,128)(2,1)S(1)} custom-call(bf16[384,512]{1,0:T(8,128)(2,1)} %q_latent.1, bf16[384,256]{1,0:T(8,128)(2,1)} %kv_latent.1, bf16[64,384]{1,0:T(8,128)(2,1)} %bitcast.5, s32[384]{0:T(512)} %doc_row.1, f32[64,3072]{1,0:T(8,128)} %constant.2.clone.table, f32[1,512]{1,0:T(1,128)} %bitcast.8, f32[1,256]{1,0:T(1,128)} %bitcast.9, ...), custom_call_target="tpu_custom_call" | custom-call | tf_op jit(solution)/shard_map/pallas_call | solution.py:1118
  125.6 0.7 copy.19
